TPU v7x, 32 devices: a whole 2x2x4 slice. The times are simulated.
32 devices in a mesh: ep: 4 (over y, x), tp: 8 (over z, core).
Axes of the slice: x: 2, y: 2, z: 4, core: 2. Of those that a mesh axis runs over, the one named last changes fastest.
Arguments:
- queries: bfloat16 [4096, 1024], P('ep', 'tp'), may hold values from -12 to 12
- keys: bfloat16 [4096, 1024], P('ep', 'tp'), may hold values from -12 to 12
- values: bfloat16 [4096, 2048], P('ep', 'tp'), may hold values from -6 to 6
- out_gate: bfloat16 [4096, 2048], P('ep', 'tp'), may hold values from -6 to 6
- in_gate: float32 [16, 4096], P('tp', 'ep'), may hold values from -8 to 100
- forget_gate: float32 [16, 4096], P('tp', 'ep'), may hold values from 0 to 16
- out_gain: float32 [2048], P('tp'), may hold values from 0.1 to 1.9
- out_weight: bfloat16 [2048, 4096], P('tp'), may hold values from -0.1875 to 0.1875
- moe_rows: bfloat16 [512, 4096], P('ep'), may hold values from -36 to 36
- moe_gain: float32 [4096], replicated, may hold values from 0.1 to 1.9
- routes: int32 [512, 2], P('ep'), may hold values from 0 to 3, all different within a row; in each aligned block of 128 rows (0 to 127, 128 to 255, ...) at most 96 rows name the same one
- route_weight: float32 [512, 2], P('ep'), may hold values from 0.2 to 1.2
- expert_gate: bfloat16 [4, 4096, 4096], P('ep', None, 'tp'), may hold values from -0.09375 to 0.09375
- expert_up: bfloat16 [4, 4096, 4096], P('ep', None, 'tp'), may hold values from -0.09375 to 0.09375
- expert_down: bfloat16 [4, 4096, 4096], P('ep', 'tp'), may hold values from -0.125 to 0.125
- shared_gate: bfloat16 [4096, 2048], P(None, 'tp'), may hold values from -0.09375 to 0.09375
- shared_up: bfloat16 [4096, 2048], P(None, 'tp'), may hold values from -0.09375 to 0.09375
- shared_down: bfloat16 [2048, 4096], P('tp'), may hold values from -0.1875 to 0.1875
Outputs:
- mixer_out: bfloat16 [4096, 4096], P('ep', 'tp')
- moe_out: bfloat16 [512, 4096], P('ep', 'tp')
Inputs may be any that keep to these rules, and one draw needn't show every extreme that they name: `routes`: each row names 2 different experts. Within the 128 rows of one index of ep no expert is named more than 96 times, a bound that some block reaches.
All inputs are finite; a program needn't handle non-finite values.
Results may differ from a plain program's by a relative error of at most 0.019.
Values may be sent and summed in bfloat16 or wider, within the bound.
A program may use at most 128 MiB of HBM per device.

v0:
```python
import functools

import jax
import jax.numpy as jnp
from jax import lax
from jax.experimental import pallas as pl
from jax.experimental.pallas import tpu as pltpu
from jax.sharding import PartitionSpec as P

DK = 64
DV = 128
CH = 128
F32 = jnp.float32
BF16 = jnp.bfloat16
VM = pl.BlockSpec(memory_space=pltpu.VMEM)


def gate_rows(ig, fg):
    lane = lax.broadcasted_iota(jnp.int32, ig.shape, 1)
    total = jnp.minimum(fg, 0.0) - jnp.log1p(jnp.exp(-jnp.abs(fg)))
    step = 1
    while step < CH:
        total = total + jnp.where(lane >= step, pltpu.roll(total, step, 1), 0.0)
        step *= 2
    level = ig - total
    top = level
    step = 1
    while step < CH:
        top = jnp.maximum(top, jnp.where(lane >= step, pltpu.roll(top, step, 1), -1e30))
        step *= 2
    return total, level, top


def columns_of(parts):
    rows = sum(part.shape[0] for part in parts)
    padded = -(-rows // 128) * 128
    if padded > rows:
        parts = list(parts) + [jnp.zeros((padded - rows, CH), F32)]
    return jnp.concatenate(parts, axis=0).T


def split_bf16(x):
    high = x.astype(BF16)
    return high, (x - high.astype(F32)).astype(BF16)


def weighted_keys(keys, cols, first, heads, chunks):
    lane_head = lax.broadcasted_iota(jnp.int32, keys.shape, 1) // DK
    weight = jnp.broadcast_to(cols[:, first : first + 1], keys.shape)
    for h in range(1, heads):
        at = first + h * chunks
        weight = jnp.where(lane_head == h, jnp.broadcast_to(cols[:, at : at + 1], keys.shape), weight)
    return split_bf16(keys.astype(F32) * weight)


def add_outer(kw, values):
    dims = (((0,), (0,)), ((), ()))
    return lax.dot_general(kw[0], values, dims, preferred_element_type=F32) + lax.dot_general(
        kw[1], values, dims, preferred_element_type=F32
    )


def pick_head(parts, shape, axis):
    head = lax.broadcasted_iota(jnp.int32, shape, axis) // DK
    out = jnp.broadcast_to(parts[0], shape)
    for h in range(1, len(parts)):
        out = jnp.where(head == h, jnp.broadcast_to(parts[h], shape), out)
    return out


def summary_kernel(heads, chunks, k_ref, v_ref, ig_ref, fg_ref, out_ref):
    width = heads * DK
    total, level, top = gate_rows(ig_ref[...], fg_ref[...])
    shape = total.shape
    chunk = lax.broadcasted_iota(jnp.int32, shape, 0) % chunks
    last = jnp.broadcast_to(total[:, CH - 1 : CH], shape)
    suffix = last
    step = 1
    while step < chunks:
        moved = pltpu.roll(suffix, shape[0] - step, 0)
        suffix = suffix + jnp.where(chunk + step < chunks, moved, 0.0)
        step *= 2
    reach = suffix + jnp.broadcast_to(top[:, CH - 1 : CH], shape)
    tops = [
        jnp.max(reach[h * chunks : (h + 1) * chunks], axis=0, keepdims=True) for h in range(heads)
    ]
    weight = [
        jnp.exp(
            level[h * chunks : (h + 1) * chunks] + suffix[h * chunks : (h + 1) * chunks] - tops[h]
        )
        for h in range(heads)
    ]
    cols = columns_of(weight)
    state = jnp.zeros((width, heads * DV + 128), F32)
    for c in range(chunks):
        rows = pl.ds(c * CH, CH)
        kw = weighted_keys(k_ref[rows, :], cols, c, heads, chunks)
        values = jnp.concatenate([v_ref[rows, :], jnp.ones((CH, 128), BF16)], axis=1)
        state = state + add_outer(kw, values)
    out_ref[...] = jnp.zeros_like(out_ref)
    out_ref[0:width, :] = pick_head(
        [state[:, h * DV : (h + 1) * DV] for h in range(heads)], (width, DV), 0
    )
    normal = state[:, heads * DV :].T
    out_ref[width : width + 1, 0:width] = normal[0:1, :]
    for h in range(heads):
        out_ref[width + 1 + h : width + 2 + h, :] = tops[h]
        at = width + 1 + heads + h
        out_ref[at : at + 1, :] = suffix[h * chunks : h * chunks + 1]


def cells_kernel(
    heads, chunks, pos_ref, q_ref, k_ref, v_ref, og_ref, ig_ref, fg_ref, gain_ref, sum_ref, out_ref
):
    width = heads * DK
    matrix = jnp.zeros((width, DV), F32)
    normal = jnp.zeros((1, width), F32)
    stab = [jnp.zeros((1, 128), F32) for _ in range(heads)]
    for e in range(sum_ref.shape[0]):
        reached = e < pos_ref[0]
        part = sum_ref.at[e]
        old_w, new_w, new_stab = [], [], []
        for h in range(heads):
            at = width + 1 + h
            carried = part[at + heads : at + heads + 1, :] + stab[h]
            there = part[at : at + 1, :]
            joined = jnp.maximum(carried, there)
            old_w.append(jnp.where(reached, jnp.exp(carried - joined), 1.0))
            new_w.append(jnp.where(reached, jnp.exp(there - joined), 0.0))
            new_stab.append(jnp.where(reached, joined, stab[h]))
        matrix = (
            pick_head(old_w, (width, DV), 0) * matrix
            + pick_head(new_w, (width, DV), 0) * part[0:width, :]
        )
        normal = (
            pick_head([w[:, 0:width] for w in old_w], (1, width), 1) * normal
            + pick_head([w[:, 0:width] for w in new_w], (1, width), 1)
            * part[width : width + 1, 0:width]
        )
        stab = new_stab
    normal_cols = jnp.broadcast_to(normal, (128, width)).T
    state = jnp.concatenate([matrix] * heads + [normal_cols], axis=1)

    total, level, top = gate_rows(ig_ref[...], fg_ref[...])
    shape = total.shape
    last = jnp.broadcast_to(total[:, CH - 1 : CH], shape)
    last_top = jnp.broadcast_to(top[:, CH - 1 : CH], shape)
    entering, leaving = [], []
    for h in range(heads):
        now = stab[h]
        for c in range(chunks):
            r = h * chunks + c
            entering.append(now)
            now = last[r : r + 1] + jnp.maximum(now, last_top[r : r + 1])
            leaving.append(now)
    entering = jnp.concatenate(entering, axis=0)
    leaving = jnp.concatenate(leaving, axis=0)
    peak = jnp.maximum(top, entering)
    decay = jnp.exp(last + entering - leaving)
    count = heads * chunks
    cols = columns_of(
        [
            peak,
            jnp.exp(entering - peak),
            jnp.exp(-(total + peak)),
            jnp.exp(last + level - leaving),
        ]
    )
    causal = lax.broadcasted_iota(jnp.int32, (CH, CH), 0) >= lax.broadcasted_iota(
        jnp.int32, (CH, CH), 1
    )
    lane_head = lax.broadcasted_iota(jnp.int32, (CH, width), 1) // DK
    for c in range(chunks):
        rows = pl.ds(c * CH, CH)
        keys = k_ref[rows, :]
        values = v_ref[rows, :]
        queries = q_ref[rows, :] * jnp.asarray(DK**-0.5, BF16)
        high, low = split_bf16(state)
        for h in range(heads):
            r = h * chunks + c
            mine = jnp.where(lane_head == h, queries, jnp.zeros_like(queries))
            raw = lax.dot_general(
                mine, keys, (((1,), (1,)), ((), ())), preferred_element_type=F32
            )
            logs = level[r : r + 1, :] - cols[:, r : r + 1]
            scores = raw * jnp.exp(jnp.where(causal, logs, -jnp.inf))
            inner = jnp.dot(
                scores.astype(BF16), values[:, h * DV : (h + 1) * DV], preferred_element_type=F32
            )
            across = 0.0
            for piece in (high, low):
                rhs = jnp.concatenate(
                    [piece[:, h * DV : (h + 1) * DV], piece[:, heads * DV :]], axis=1
                )
                across = across + jnp.dot(mine, rhs, preferred_element_type=F32)
            inter = cols[:, count + r : count + r + 1]
            signed = jnp.sum(scores, axis=1, keepdims=True) + inter * across[:, DV : DV + 1]
            divisor = jnp.maximum(jnp.abs(signed), cols[:, 2 * count + r : 2 * count + r + 1])
            cells = (inner + inter * across[:, :DV]) * (1.0 / divisor)
            at = slice(h * DV, (h + 1) * DV)
            gate = og_ref[rows, at].astype(F32)
            out_ref[rows, at] = (cells / (1.0 + jnp.exp(-gate)) * gain_ref[:, at]).astype(BF16)
        if c + 1 < chunks:
            kw = weighted_keys(keys, cols, 3 * count + c, heads, chunks)
            scale = pick_head(
                [decay[h * chunks + c : h * chunks + c + 1] for h in range(heads)], (width, 128), 0
            )
            rhs = jnp.concatenate([values, jnp.ones((CH, 128), BF16)], axis=1)
            state = state * jnp.concatenate([scale] * (heads + 1), axis=1) + add_outer(kw, rhs)


def mixed_cells(queries, keys, values, out_gate, in_gate, forget_gate, out_gain):
    tok_rows = queries.shape[0]
    heads = in_gate.shape[0]
    chunks = tok_rows // CH
    width = heads * DK
    ig = in_gate.reshape(heads * chunks, CH)
    fg = forget_gate.reshape(heads * chunks, CH)
    extra = -(-(1 + 2 * heads) // 8) * 8
    summary = pl.pallas_call(
        functools.partial(summary_kernel, heads, chunks),
        out_shape=jax.ShapeDtypeStruct((width + extra, 128), F32),
        in_specs=[VM] * 4,
        out_specs=VM,
        cost_estimate=pl.CostEstimate(flops=400_000_000, bytes_accessed=8_000_000, transcendentals=0),
    )(keys, values, ig, fg)
    everything = lax.all_gather(summary, "ep")
    pos = lax.axis_index("ep").astype(jnp.int32).reshape(1)
    return pl.pallas_call(
        functools.partial(cells_kernel, heads, chunks),
        out_shape=jax.ShapeDtypeStruct((tok_rows, heads * DV), BF16),
        in_specs=[pl.BlockSpec(memory_space=pltpu.SMEM)] + [VM] * 8,
        out_specs=VM,
        cost_estimate=pl.CostEstimate(flops=2_000_000_000, bytes_accessed=16_000_000, transcendentals=0),
    )(pos, queries, keys, values, out_gate, ig, fg, out_gain.reshape(1, -1), everything)


def mixer_kernel(a_ref, w_ref, out_ref):
    width = a_ref.shape[2]
    total = jnp.dot(a_ref[0], w_ref[0:width, :], preferred_element_type=F32)
    for i in range(1, a_ref.shape[0]):
        total = total + jnp.dot(
            a_ref[i], w_ref[i * width : (i + 1) * width, :], preferred_element_type=F32
        )
    out_ref[...] = total.astype(out_ref.dtype)


def mixer(gathered, weight):
    parts, rows, width = gathered.shape
    cols = weight.shape[1]
    tile = min(256, rows)
    return pl.pallas_call(
        mixer_kernel,
        grid=(rows // tile,),
        out_shape=jax.ShapeDtypeStruct((rows, cols), BF16),
        in_specs=[
            pl.BlockSpec((parts, tile, width), lambda r: (0, r, 0)),
            pl.BlockSpec((parts * width, cols), lambda r: (0, 0)),
        ],
        out_specs=pl.BlockSpec((tile, cols), lambda r: (r, 0)),
        cost_estimate=pl.CostEstimate(
            flops=2 * rows * parts * width * cols, bytes_accessed=8_000_000, transcendentals=0
        ),
    )(gathered, weight)


def hidden_kernel(x_ref, g_ref, u_ref, out_ref, gate_acc, up_acc):
    k = pl.program_id(0)
    x = x_ref[...]
    gate = jnp.dot(x, g_ref[...], preferred_element_type=F32)
    up = jnp.dot(x, u_ref[...], preferred_element_type=F32)

    @pl.when(k == 0)
    def _():
        gate_acc[...] = gate
        up_acc[...] = up

    @pl.when(k > 0)
    def _():
        gate_acc[...] += gate
        up_acc[...] += up

    @pl.when(k == pl.num_programs(0) - 1)
    def _():
        g = gate_acc[...]
        out_ref[...] = (g / (1.0 + jnp.exp(-g)) * up_acc[...]).astype(BF16)


def hidden_units(x, w_gate, w_up):
    rows, depth = x.shape
    cols = w_gate.shape[1]
    tile = min(512, depth)
    return pl.pallas_call(
        hidden_kernel,
        grid=(depth // tile,),
        out_shape=jax.ShapeDtypeStruct((rows, cols), BF16),
        in_specs=[
            pl.BlockSpec((rows, tile), lambda k: (0, k)),
            pl.BlockSpec((tile, cols), lambda k: (k, 0)),
            pl.BlockSpec((tile, cols), lambda k: (k, 0)),
        ],
        out_specs=pl.BlockSpec((rows, cols), lambda k: (0, 0)),
        scratch_shapes=[pltpu.VMEM((rows, cols), F32)] * 2,
        cost_estimate=pl.CostEstimate(
            flops=4 * rows * depth * cols,
            bytes_accessed=2 * depth * (rows + 2 * cols),
            transcendentals=0,
        ),
    )(x, w_gate, w_up)


def down_kernel(h_ref, d_ref, sh_ref, sd_ref, out_ref):
    slots = h_ref.shape[0]
    out_ref[0, 0:slots, :] = jnp.dot(h_ref[...], d_ref[...], preferred_element_type=F32).astype(BF16)
    out_ref[0, slots:, :] = jnp.dot(sh_ref[...], sd_ref[...], preferred_element_type=F32).astype(
        BF16
    )


def down_parts(hidden, w_down, shared_hidden, shared_down, blocks):
    slots, depth = hidden.shape
    shared_rows, shared_depth = shared_hidden.shape
    feat = w_down.shape[1] // blocks
    rows = slots + shared_rows
    return pl.pallas_call(
        down_kernel,
        grid=(blocks,),
        out_shape=jax.ShapeDtypeStruct((blocks, rows, feat), BF16),
        in_specs=[
            pl.BlockSpec((slots, depth), lambda j: (0, 0)),
            pl.BlockSpec((depth, feat), lambda j: (0, j)),
            pl.BlockSpec((shared_rows, shared_depth), lambda j: (0, 0)),
            pl.BlockSpec((shared_depth, feat), lambda j: (0, j)),
        ],
        out_specs=pl.BlockSpec((1, rows, feat), lambda j: (j, 0, 0)),
        cost_estimate=pl.CostEstimate(
            flops=2 * slots * depth * feat * blocks, bytes_accessed=10_000_000, transcendentals=0
        ),
    )(hidden, w_down, shared_hidden, shared_down)


def weight_columns(out_weight):
    tp_count, ep_count = lax.axis_size("tp"), lax.axis_size("ep")
    depth, features = out_weight.shape
    mine = features // tp_count
    share = mine // ep_count
    part = lax.dynamic_index_in_dim(
        out_weight.reshape(depth, tp_count, ep_count, share), lax.axis_index("ep"), 2, False
    )
    part = part.transpose(1, 0, 2)
    part = lax.all_to_all(part, "tp", split_axis=0, concat_axis=0, tiled=True)
    whole = lax.all_gather(part.reshape(tp_count * depth, share), "ep")
    return whole.transpose(1, 0, 2).reshape(tp_count * depth, mine)


def local(
    queries,
    keys,
    values,
    out_gate,
    in_gate,
    forget_gate,
    out_gain,
    out_weight,
    moe_rows,
    moe_gain,
    routes,
    route_weight,
    expert_gate,
    expert_up,
    expert_down,
    shared_gate,
    shared_up,
    shared_down,
):
    tp_count = lax.axis_size("tp")
    ep_count = lax.axis_size("ep")
    routed_rows, topk_count = routes.shape
    local_experts = expert_gate.shape[0]
    assert local_experts == 1
    expert_count = local_experts * ep_count
    capacity = 3 * routed_rows * topk_count // (2 * expert_count)
    slot_count = expert_count * capacity

    rows_wide = moe_rows.astype(F32)
    inverse = lax.rsqrt(jnp.mean(rows_wide * rows_wide, axis=1, keepdims=True) + 1e-06)
    normed = (rows_wide * inverse * moe_gain).astype(BF16)
    flat_routes = routes.reshape(-1)
    count = flat_routes.shape[0]
    onehot = flat_routes[:, None] == jnp.arange(expert_count, dtype=jnp.int32)[None, :]
    earlier = jnp.tril(jnp.ones((count, count), BF16), -1)
    before = jnp.dot(earlier, onehot.astype(BF16), preferred_element_type=F32)
    token_position = jnp.sum(jnp.where(onehot, before, 0.0), axis=1).astype(jnp.int32)
    destination = (flat_routes * capacity + token_position).reshape(routed_rows, topk_count)
    slots = jnp.arange(slot_count, dtype=jnp.int32)
    hit = destination[:, :, None] == slots[None, None, :]
    place = jnp.any(hit, axis=1).astype(BF16)
    outgoing = lax.dot_general(
        place, normed, (((0,), (0,)), ((), ())), preferred_element_type=F32
    ).astype(BF16)
    arrived = lax.all_to_all(outgoing, "ep", split_axis=0, concat_axis=0, tiled=True)

    out_columns = weight_columns(out_weight)
    mixed = mixed_cells(queries, keys, values, out_gate, in_gate, forget_gate, out_gain)
    gathered = lax.all_gather(mixed, "tp")

    shared_hidden = hidden_units(normed, shared_gate, shared_up)
    hidden = hidden_units(arrived, expert_gate[0], expert_up[0])
    parts = down_parts(hidden, expert_down[0], shared_hidden, shared_down, tp_count)
    total_rows = parts.shape[1]
    summed = lax.psum_scatter(
        parts.reshape(tp_count * total_rows, parts.shape[2]), "tp", scatter_dimension=0, tiled=True
    )
    returned = lax.all_to_all(summed[:slot_count], "ep", split_axis=0, concat_axis=0, tiled=True)
    weights = jnp.sum(jnp.where(hit, route_weight[:, :, None], 0.0), axis=1)
    picked = jnp.dot(
        weights, returned.astype(F32), precision=lax.Precision.HIGHEST, preferred_element_type=F32
    )
    moe_out = (picked + summed[slot_count:].astype(F32)).astype(BF16)
    mixer_out = mixer(gathered, out_columns)
    return (mixer_out, moe_out)


def solution(mesh):
    return jax.shard_map(
        local,
        mesh=mesh,
        in_specs=(
            P("ep", "tp"),
            P("ep", "tp"),
            P("ep", "tp"),
            P("ep", "tp"),
            P("tp", "ep"),
            P("tp", "ep"),
            P("tp"),
            P("tp", None),
            P("ep", None),
            P(),
            P("ep", None),
            P("ep", None),
            P("ep", None, "tp"),
            P("ep", None, "tp"),
            P("ep", "tp", None),
            P(None, "tp"),
            P(None, "tp"),
            P("tp", None),
        ),
        out_specs=(P("ep", "tp"), P("ep", "tp")),
        check_vma=False,
    )
```

profile of v0, /device:TPU:0, one launch (start us, length us, event | category | flops | bytes accessed | tf_op | source)
XLA Modules:
  0.0 213.3 jit_solution(810017691300656158)
XLA Ops:
  8.0 1.6 fusion
  9.6 0.8 copy.56
  10.4 0.1 eq.28
  10.6 0.3 fusion.4
  10.8 0.1 convert_element_type.27
  11.0 0.7 multiply_add_fusion
  11.8 0.1 fusion.5
  11.9 1.0 fusion.2.x_ref
  12.9 2.7 %convolution_convert_fusion = bf16[384,4096]{1,0:T(8,128)(2,1)} fusion(pred[128,384]{1,0:T(8,128)(4,1)S(1)} %fusion.5, bf16[128,4096]{1,0:T(8,128)(2,1)S(1)} %fusion.2.x_ref), kind=kOutput, calls=%fused_computation | convolution fusion | flops 404226048 | bytes 4243456 | tf_op jit(solution)/shard_map/dot_general | solution.py:398
  15.6 5.2 %all-to-all-start.1 = ((bf16[4,96,4096]{2,1,0:T(8,128)(2,1)}), bf16[4,96,4096]{2,1,0:T(8,128)(2,1)S(1)}, u32[]{:S(2)}, u32[]{:S(2)}) async-start(bf16[4,96,4096]{2,1,0:T(8,128)(2,1)} %bitcast.10), calls=%async_computation.1 | async-start | bytes 6291456 | tf_op jit(solution)/shard_map/all_to_all | solution.py:401
  20.8 6.5 %shard_map.189.sh_ref = bf16[128,256]{1,0:T(8,128)(2,1)} custom-call(bf16[128,4096]{1,0:T(8,128)(2,1)} %copy-done.1, bf16[4096,256]{1,0:T(8,128)(2,1)} %g_ref.1, bf16[4096,256]{1,0:T(8,128)(2,1)} %u_ref.1), custom_call_target="tpu_custom_call" | custom-call | flops 536870912 | bytes 5242880 | tf_op jit(solution)/shard_map/pallas_call | solution.py:293
  27.3 29.6 %all-to-all-done.1 = bf16[4,96,4096]{2,1,0:T(8,128)(2,1)S(1)} async-done(((bf16[4,96,4096]{2,1,0:T(8,128)(2,1)}), bf16[4,96,4096]{2,1,0:T(8,128)(2,1)S(1)}, u32[]{:S(2)}, u32[]{:S(2)}) %all-to-all-start.1) | async-done | bytes 3145760 | tf_op jit(solution)/shard_map/all_to_all | solution.py:401
  56.9 1.6 copy-done
  58.6 10.1 %shard_map.188.h_ref = bf16[384,512]{1,0:T(8,128)(2,1)} custom-call(bf16[384,4096]{1,0:T(8,128)(2,1)} %bitcast.29, bf16[4096,512]{1,0:T(8,128)(2,1)} %bitcast.30, bf16[4096,512]{1,0:T(8,128)(2,1)} %bitcast.31), custom_call_target="tpu_custom_call" | custom-call | flops 3221225472 | bytes 11534336 | tf_op jit(solution)/shard_map/pallas_call | solution.py:293
  68.7 8.4 %shard_map.190 = bf16[8,512,512]{2,1,0:T(8,128)(2,1)} custom-call(bf16[384,512]{1,0:T(8,128)(2,1)} %shard_map.188.h_ref, bf16[512,4096]{1,0:T(8,128)(2,1)} %bitcast.32, bf16[128,256]{1,0:T(8,128)(2,1)} %shard_map.189.sh_ref, bf16[256,4096]{1,0:T(8,128)(2,1)} %sd_ref.1), custom_call_target="tpu_custom_call" | custom-call | flops 1610612736 | bytes 10000000 | tf_op jit(solution)/shard_map/pallas_call | solution.py:325
  77.2 3.3 %copy.52 = bf16[256,4096]{0,1:T(8,128)(2,1)S(1)} copy(bf16[256,4096]{1,0:T(8,128)(2,1)} %param.25) | data formatting | bytes 4194304 | tf_op args[7]
  80.5 0.3 copy.54
  80.8 29.1 %all_to_all.28 = bf16[8,256,128]{2,1,0:T(8,128)(2,1)} all-to-all(bf16[8,256,128]{2,1,0:T(8,128)(2,1)S(1)} %copy.54), channel_id=1, replica_groups=mesh['ep'=4,'tp'=8] {'tp'}, dimensions={0} | all-to-all | bytes 1048576 | tf_op jit(solution)/shard_map/all_to_all | solution.py:351
  110.0 0.6 reshape.50.ig_ref
  110.6 0.6 reshape.51.fg_ref
  111.2 3.9 %shard_map.185 = f32[136,128]{1,0:T(8,128)} custom-call(bf16[1024,128]{1,0:T(8,128)(2,1)} %k_ref.3, bf16[1024,256]{1,0:T(8,128)(2,1)} %v_ref.3, f32[16,128]{1,0:T(8,128)} %reshape.50.ig_ref, f32[16,128]{1,0:T(8,128)} %reshape.51.fg_ref), custom_call_target="tpu_custom_call" | custom-call | flops 400000000 | bytes 8000000 | tf_op jit(solution)/shard_map/pallas_call | solution.py:220
  115.1 11.2 %all-gather = f32[544,128]{1,0:T(8,128)} all-gather(f32[136,128]{1,0:T(8,128)} %shard_map.185), channel_id=2, replica_groups=mesh['ep'=4,'tp'=8] {'ep'}, dimensions={0}, use_global_device_ids=true | all-gather | bytes 348160 | tf_op jit(solution)/shard_map/all_gather | solution.py:227
  126.3 7.2 %shard_map.186 = bf16[1024,256]{1,0:T(8,128)(2,1)} custom-call(s32[1]{0:T(128)} %bitcast.pos_ref, bf16[1024,128]{1,0:T(8,128)(2,1)} %q_ref.1, bf16[1024,128]{1,0:T(8,128)(2,1)} %k_ref.3, bf16[1024,256]{1,0:T(8,128)(2,1)} %v_ref.3, bf16[1024,256]{1,0:T(8,128)(2,1)} %og_ref.1, f32[16,128]{1,0:T(8,128)} %reshape.50.ig_ref, f32[16,128]{1,0:T(8,128)} %reshape.51.fg_ref, ...), custom_call_target="tpu_custom_call" | custom-call | flops 2000000000 | bytes 16000000 | tf_op jit(solution)/shard_map/pallas_call | solution.py:229
  133.5 0.1 select_reduce_fusion
  133.7 2.4 %reduce-scatter.2.cloned.1.call-done = bf16[512,512]{1,0:T(8,128)(2,1)} async-done(((bf16[4096,512]{1,0:T(8,128)(2,1)}), bf16[512,512]{1,0:T(8,128)(2,1)}) %reduce-scatter.2.cloned.1.call-update) | async-done | bytes 524304 | tf_op jit(solution)/shard_map/reduce_scatter | solution.py:411
  136.1 1.8 slice.8
  137.9 3.6 %all-to-all-start.2 = ((bf16[4,96,512]{2,1,0:T(8,128)(2,1)}), bf16[4,96,512]{2,1,0:T(8,128)(2,1)S(1)}, u32[]{:S(2)}, u32[]{:S(2)}) async-start(bf16[4,96,512]{2,1,0:T(8,128)(2,1)} %bitcast.16), calls=%async_computation.3 | async-start | bytes 786432 | tf_op jit(solution)/shard_map/all_to_all | solution.py:414
  141.5 7.0 %all-gather.5.cloned.1.call-done = bf16[4,2048,128]{2,1,0:T(8,128)(2,1)} async-done(((bf16[1,2048,128]{2,1,0:T(8,128)(2,1)}), bf16[4,2048,128]{2,1,0:T(8,128)(2,1)}) %all-gather.5.cloned.1.call-update) | async-done | bytes 2097168 | tf_op jit(solution)/shard_map/all_gather | solution.py:352
  148.5 3.1 %copy_bitcast_fusion.w_ref = bf16[2048,512]{1,0:T(8,128)(2,1)} fusion(bf16[4,2048,128]{2,1,0:T(8,128)(2,1)} %all-gather.5.cloned.1.call-done), kind=kLoop, calls=%fused_computation.6 | loop fusion | bytes 4194304 | tf_op jit(solution)/shard_map/reshape | solution.py:353
  151.7 46.1 %all-gather.7.cloned.1.call-done = bf16[8192,256]{1,0:T(8,128)(2,1)} async-done(((bf16[1024,256]{1,0:T(8,128)(2,1)}), bf16[8192,256]{1,0:T(8,128)(2,1)}) %all-gather.7.cloned.1.call-update) | async-done | bytes 4194320 | tf_op jit(solution)/shard_map/all_gather | solution.py:405
  197.8 6.2 %shard_map.187 = bf16[1024,512]{1,0:T(8,128)(2,1)} custom-call(bf16[8,1024,256]{2,1,0:T(8,128)(2,1)} %bitcast.37, bf16[2048,512]{1,0:T(8,128)(2,1)} %copy_bitcast_fusion.w_ref), custom_call_target="tpu_custom_call" | custom-call | flops 2147483648 | bytes 8000000 | tf_op jit(solution)/shard_map/pallas_call | solution.py:252
  203.9 1.9 fusion.3
  (23 shorter events, 0.3 us)
Async XLA Ops:
  8.0 3.9 %copy-start.2 = (bf16[128,4096]{1,0:T(8,128)(2,1)S(1)}, bf16[128,4096]{1,0:T(8,128)(2,1)}, u32[]{:S(2)}) copy-start(bf16[128,4096]{1,0:T(8,128)(2,1)} %param.26) | copy-start | bytes 3145732
  12.9 2.7 %copy-start.1 = (bf16[128,4096]{1,0:T(8,128)(2,1)}, bf16[128,4096]{1,0:T(8,128)(2,1)S(1)}, u32[]{:S(2)}) copy-start(bf16[128,4096]{1,0:T(8,128)(2,1)S(1)} %fusion.2.x_ref) | copy-start | bytes 3145732
  15.6 41.3 %all-to-all-start.1 = ((bf16[4,96,4096]{2,1,0:T(8,128)(2,1)}), bf16[4,96,4096]{2,1,0:T(8,128)(2,1)S(1)}, u32[]{:S(2)}, u32[]{:S(2)}) async-start(bf16[4,96,4096]{2,1,0:T(8,128)(2,1)} %bitcast.10), calls=%async_computation.1 | async-start | bytes 6291456 | tf_op jit(solution)/shard_map/all_to_all | solution.py:401
  20.8 115.3 %reduce-scatter.2.cloned.1.call-start = ((), (), s32[]{:S(2)}) async-start(), calls=%async_computation.5 | async-start | bytes 4718592 | tf_op jit(solution)/shard_map/reduce_scatter | solution.py:411
  56.9 1.6 copy-start
  77.1 71.4 %all-gather.5.cloned.1.call-start = ((), (), s32[]{:S(2)}) async-start(), calls=%async_computation.4 | async-start | bytes 2621440 | tf_op jit(solution)/shard_map/all_gather | solution.py:352
  80.4 29.5 %copy-start.3 = (f32[2,1024]{1,0:T(2,128)S(1)}, f32[2,1024]{1,0:T(2,128)}, u32[]{:S(2)}) copy-start(f32[2,1024]{1,0:T(2,128)} %param.22) | copy-start | bytes 24580
  80.5 30.1 %copy-start.4 = (f32[2,1024]{1,0:T(2,128)S(1)}, f32[2,1024]{1,0:T(2,128)}, u32[]{:S(2)}) copy-start(f32[2,1024]{1,0:T(2,128)} %param.23) | copy-start | bytes 24580
  109.9 87.8 %all-gather.7.cloned.1.call-start = ((), (), s32[]{:S(2)}) async-start(), calls=%async_computation.6 | async-start | bytes 4718592 | tf_op jit(solution)/shard_map/all_gather | solution.py:405
  126.3 7.2 %copy-start.5 = (f32[128,2]{0,1:T(2,128)S(1)}, f32[128,2]{0,1:T(2,128)}, u32[]{:S(2)}) copy-start(f32[128,2]{0,1:T(2,128)} %param.29) | copy-start | bytes 3076
  137.9 66.1 %all-to-all-start.2 = ((bf16[4,96,512]{2,1,0:T(8,128)(2,1)}), bf16[4,96,512]{2,1,0:T(8,128)(2,1)S(1)}, u32[]{:S(2)}, u32[]{:S(2)}) async-start(bf16[4,96,512]{2,1,0:T(8,128)(2,1)} %bitcast.16), calls=%async_computation.3 | async-start | bytes 786432 | tf_op jit(solution)/shard_map/all_to_all | solution.py:414
Sparse Core Ops, SparseCore 0:
  77.2 58.8 reduce-scatter.1
Sparse Core Ops, SparseCore 1:
  110.0 38.5 all-gather.4
  150.6 47.1 all-gather.6
where the time goes:
time: 215 us; the launch traced here: 213 us
  waiting for transfers between devices  85.2 us (40%)
  Pallas kernels  42.2 us (20%)
  blocking collectives  40.3 us (19%)
  between operations  15.6 us (7%)
  local copies, waits for them, and re-layouts  12.5 us (6%)
  starting transfers between devices  8.93 us (4%)
  matrix products  4.88 us (2%)
  other arithmetic  3.61 us (2%)
    all_gather x1, waiting for transfers between devices, local(): gathered = lax.all_gather(mixed, 'tp')  46.1 us
    all_to_all x1, waiting for transfers between devices, local(): lax.all_to_all(outgoing, 'ep', split_axis=0, concat_axis=0, tiled=True)  29.6 us
    all_to_all x1, blocking collectives, weight_columns(): part = lax.all_to_all(part, 'tp', split_axis=0, concat_axis=0, tiled=True)  29.1 us
    pallas_call x2, Pallas kernels, hidden_units(): pl.pallas_call(hidden_kernel, grid=(depth // tile,), out_shape=jax.ShapeD...  16.6 us
    all_gather x1, blocking collectives, mixed_cells(): everything = lax.all_gather(summary, 'ep')  11.2 us
    pallas_call x1, Pallas kernels, down_parts(): pl.pallas_call(down_kernel, grid=(blocks,), out_shape=jax.ShapeDtypeStruc...  8.37 us
    pallas_call x1, Pallas kernels, mixed_cells(): pl.pallas_call(functools.partial(cells_kernel, heads, chunks), out_shape=...  7.17 us
    all_gather x1, waiting for transfers between devices, weight_columns(): whole = lax.all_gather(part.reshape(tp_count * depth, share), 'ep')  7.03 us
  transfers between devices with their start and end apart: 5, of which 4 were waited for; matrix products, arithmetic and copies ran while one was open for 5% of the time, Pallas kernels for 11%

commit v1 on v0

v1 whole, which is shorter than its diff:
```python
import functools

import jax
import jax.numpy as jnp
from jax import lax
from jax.experimental import pallas as pl
from jax.experimental.pallas import tpu as pltpu
from jax.sharding import PartitionSpec as P

DK = 64
DV = 128
CH = 128
F32 = jnp.float32
BF16 = jnp.bfloat16
VM = pl.BlockSpec(memory_space=pltpu.VMEM)
ANY = pl.BlockSpec(memory_space=pl.ANY)
MESH = pl.DeviceIdType.MESH
SPLIT = 2


def gate_rows(ig, fg):
    lane = lax.broadcasted_iota(jnp.int32, ig.shape, 1)
    total = jnp.minimum(fg, 0.0) - jnp.log1p(jnp.exp(-jnp.abs(fg)))
    step = 1
    while step < CH:
        total = total + jnp.where(lane >= step, pltpu.roll(total, step, 1), 0.0)
        step *= 2
    level = ig - total
    top = level
    step = 1
    while step < CH:
        top = jnp.maximum(top, jnp.where(lane >= step, pltpu.roll(top, step, 1), -1e30))
        step *= 2
    return total, level, top


def columns_of(parts):
    rows = sum(part.shape[0] for part in parts)
    padded = -(-rows // 128) * 128
    if padded > rows:
        parts = list(parts) + [jnp.zeros((padded - rows, CH), F32)]
    return jnp.concatenate(parts, axis=0).T


def split_bf16(x):
    high = x.astype(BF16)
    return high, (x - high.astype(F32)).astype(BF16)


def weighted_keys(keys, cols, first, heads, chunks):
    lane_head = lax.broadcasted_iota(jnp.int32, keys.shape, 1) // DK
    weight = jnp.broadcast_to(cols[:, first : first + 1], keys.shape)
    for h in range(1, heads):
        at = first + h * chunks
        weight = jnp.where(lane_head == h, jnp.broadcast_to(cols[:, at : at + 1], keys.shape), weight)
    return split_bf16(keys.astype(F32) * weight)


def add_outer(kw, values):
    dims = (((0,), (0,)), ((), ()))
    return lax.dot_general(kw[0], values, dims, preferred_element_type=F32) + lax.dot_general(
        kw[1], values, dims, preferred_element_type=F32
    )


def pick_head(parts, shape, axis):
    head = lax.broadcasted_iota(jnp.int32, shape, axis) // DK
    out = jnp.broadcast_to(parts[0], shape)
    for h in range(1, len(parts)):
        out = jnp.where(head == h, jnp.broadcast_to(parts[h], shape), out)
    return out


def summary(heads, chunks, k_ref, v_ref, gates, out_ref, slot):
    width = heads * DK
    total, level, top = gates
    shape = total.shape
    chunk = lax.broadcasted_iota(jnp.int32, shape, 0) % chunks
    last = jnp.broadcast_to(total[:, CH - 1 : CH], shape)
    suffix = last
    step = 1
    while step < chunks:
        moved = pltpu.roll(suffix, shape[0] - step, 0)
        suffix = suffix + jnp.where(chunk + step < chunks, moved, 0.0)
        step *= 2
    reach = suffix + jnp.broadcast_to(top[:, CH - 1 : CH], shape)
    tops = [
        jnp.max(reach[h * chunks : (h + 1) * chunks], axis=0, keepdims=True) for h in range(heads)
    ]
    weight = [
        jnp.exp(
            level[h * chunks : (h + 1) * chunks] + suffix[h * chunks : (h + 1) * chunks] - tops[h]
        )
        for h in range(heads)
    ]
    cols = columns_of(weight)
    state = jnp.zeros((width, heads * DV + 128), F32)
    for c in range(chunks):
        rows = pl.ds(c * CH, CH)
        kw = weighted_keys(k_ref[rows, :], cols, c, heads, chunks)
        values = jnp.concatenate([v_ref[rows, :], jnp.ones((CH, 128), BF16)], axis=1)
        state = state + add_outer(kw, values)
    out_ref[slot] = jnp.zeros(out_ref.shape[1:], F32)
    out_ref[slot, 0:width, :] = pick_head(
        [state[:, h * DV : (h + 1) * DV] for h in range(heads)], (width, DV), 0
    )
    normal = state[:, heads * DV :].T
    out_ref[slot, width : width + 1, 0:width] = normal[0:1, :]
    for h in range(heads):
        out_ref[slot, width + 1 + h : width + 2 + h, :] = tops[h]
        at = width + 1 + heads + h
        out_ref[slot, at : at + 1, :] = suffix[h * chunks : h * chunks + 1]


def entering_state(heads, pos, sum_ref):
    width = heads * DK
    matrix = jnp.zeros((width, DV), F32)
    normal = jnp.zeros((1, width), F32)
    stab = [jnp.zeros((1, 128), F32) for _ in range(heads)]
    for e in range(sum_ref.shape[0]):
        reached = e < pos
        part = sum_ref.at[e]
        old_w, new_w, new_stab = [], [], []
        for h in range(heads):
            at = width + 1 + h
            carried = part[at + heads : at + heads + 1, :] + stab[h]
            there = part[at : at + 1, :]
            joined = jnp.maximum(carried, there)
            old_w.append(jnp.where(reached, jnp.exp(carried - joined), 1.0))
            new_w.append(jnp.where(reached, jnp.exp(there - joined), 0.0))
            new_stab.append(jnp.where(reached, joined, stab[h]))
        matrix = (
            pick_head(old_w, (width, DV), 0) * matrix
            + pick_head(new_w, (width, DV), 0) * part[0:width, :]
        )
        normal = (
            pick_head([w[:, 0:width] for w in old_w], (1, width), 1) * normal
            + pick_head([w[:, 0:width] for w in new_w], (1, width), 1)
            * part[width : width + 1, 0:width]
        )
        stab = new_stab
    normal_cols = jnp.broadcast_to(normal, (128, width)).T
    return jnp.concatenate([matrix] * heads + [normal_cols], axis=1), stab


def cell_blocks(
    heads, chunks, state, stab, gates, q_ref, k_ref, v_ref, og_ref, gain_ref, out_ref, after
):
    width = heads * DK
    total, level, top = gates
    shape = total.shape
    last = jnp.broadcast_to(total[:, CH - 1 : CH], shape)
    last_top = jnp.broadcast_to(top[:, CH - 1 : CH], shape)
    entering, leaving = [], []
    for h in range(heads):
        now = stab[h]
        for c in range(chunks):
            r = h * chunks + c
            entering.append(now)
            now = last[r : r + 1] + jnp.maximum(now, last_top[r : r + 1])
            leaving.append(now)
    entering = jnp.concatenate(entering, axis=0)
    leaving = jnp.concatenate(leaving, axis=0)
    peak = jnp.maximum(top, entering)
    decay = jnp.exp(last + entering - leaving)
    count = heads * chunks
    cols = columns_of(
        [
            peak,
            jnp.exp(entering - peak),
            jnp.exp(-(total + peak)),
            jnp.exp(last + level - leaving),
        ]
    )
    causal = lax.broadcasted_iota(jnp.int32, (CH, CH), 0) >= lax.broadcasted_iota(
        jnp.int32, (CH, CH), 1
    )
    lane_head = lax.broadcasted_iota(jnp.int32, (CH, width), 1) // DK
    for c in range(chunks):
        rows = pl.ds(c * CH, CH)
        keys = k_ref[rows, :]
        values = v_ref[rows, :]
        queries = q_ref[rows, :] * jnp.asarray(DK**-0.5, BF16)
        high, low = split_bf16(state)
        for h in range(heads):
            r = h * chunks + c
            mine = jnp.where(lane_head == h, queries, jnp.zeros_like(queries))
            raw = lax.dot_general(
                mine, keys, (((1,), (1,)), ((), ())), preferred_element_type=F32
            )
            logs = level[r : r + 1, :] - cols[:, r : r + 1]
            scores = raw * jnp.exp(jnp.where(causal, logs, -jnp.inf))
            inner = jnp.dot(
                scores.astype(BF16), values[:, h * DV : (h + 1) * DV], preferred_element_type=F32
            )
            across = 0.0
            for piece in (high, low):
                rhs = jnp.concatenate(
                    [piece[:, h * DV : (h + 1) * DV], piece[:, heads * DV :]], axis=1
                )
                across = across + jnp.dot(mine, rhs, preferred_element_type=F32)
            inter = cols[:, count + r : count + r + 1]
            signed = jnp.sum(scores, axis=1, keepdims=True) + inter * across[:, DV : DV + 1]
            divisor = jnp.maximum(jnp.abs(signed), cols[:, 2 * count + r : 2 * count + r + 1])
            cells = (inner + inter * across[:, :DV]) * (1.0 / divisor)
            at = slice(h * DV, (h + 1) * DV)
            gate = og_ref[rows, at].astype(F32)
            out_ref[rows, at] = (cells / (1.0 + jnp.exp(-gate)) * gain_ref[:, at]).astype(BF16)
        if c + 1 < chunks:
            kw = weighted_keys(keys, cols, 3 * count + c, heads, chunks)
            scale = pick_head(
                [decay[h * chunks + c : h * chunks + c + 1] for h in range(heads)], (width, 128), 0
            )
            rhs = jnp.concatenate([values, jnp.ones((CH, 128), BF16)], axis=1)
            state = state * jnp.concatenate([scale] * (heads + 1), axis=1) + add_outer(kw, rhs)
        after(c)


def tiles(width, most):
    return min(width, most)


def step_kernel(
    ep_count,
    tp_count,
    side,
    cap,
    q_ref,
    k_ref,
    v_ref,
    og_ref,
    ig_ref,
    fg_ref,
    gain_ref,
    rows_ref,
    mg_ref,
    routes_ref,
    rw_ref,
    ow_hbm,
    eg_hbm,
    eu_hbm,
    ed_hbm,
    sg_hbm,
    su_hbm,
    sd_hbm,
    mixer_out,
    moe_out,
    sums,
    own,
    mixed,
    wcols,
    normed,
    staged,
    arrived,
    eg,
    eu,
    ed,
    sg,
    su,
    sd,
    hidden,
    shared_hidden,
    give,
    take,
    reduced,
    returned,
    shared_own,
    part_out,
    part_in,
    final,
    load_sem,
    wz_s,
    wz_r,
    wx_s,
    wx_r,
    st_s,
    st_r,
    dx_s,
    dx_r,
    dp_s,
    dp_r,
    up_s,
    up_r,
    dn_s,
    dn_r,
    pa_s,
    pa_r,
    pp_s,
    pp_r,
    rt_s,
    rt_r,
    zs_s,
    zs_r,
):
    e, t = lax.axis_index("ep"), lax.axis_index("tp")
    z, core = t // 2, t % 2
    chips = tp_count // 2
    heads = ig_ref.shape[0]
    tok = q_ref.shape[0]
    chunks = tok // CH
    count, depth = rows_ref.shape
    half = depth // 2
    feat = mixer_out.shape[1]
    share = wcols.shape[2]
    slots = ep_count * cap
    group = tp_count // SPLIT
    seg = tok // SPLIT

    def ep_peer(dy, dx):
        deep = ep_count // side
        return ((e // side + dy) % deep) * side + (e % side + dx) % side

    around = [(dy, dx) for dy in range(ep_count // side) for dx in range(side)][1:]
    around = around[::-1]

    def remote(src, dst, send, recv, where):
        return pltpu.make_async_remote_copy(
            src_ref=src, dst_ref=dst, send_sem=send, recv_sem=recv, device_id=where,
            device_id_type=MESH,
        )

    loads = [
        pltpu.make_async_copy(src, dst, load_sem.at[i])
        for i, (src, dst) in enumerate(
            [
                (sg_hbm, sg),
                (su_hbm, su),
                (eg_hbm.at[0], eg),
                (eu_hbm.at[0], eu),
                (ed_hbm.at[0], ed),
                (sd_hbm, sd),
                (
                    ow_hbm.at[
                        pl.ds(pl.multiple_of(e * share, share), share),
                        pl.ds(pl.multiple_of(t * feat, feat), feat),
                    ],
                    wcols.at[t, e],
                ),
            ]
        )
    ]
    barrier = pltpu.get_barrier_semaphore()
    for dy, dx in around:
        pl.semaphore_signal(barrier, inc=1, device_id=(ep_peer(dy, dx), t), device_id_type=MESH)
    for k in range(1, tp_count):
        pl.semaphore_signal(
            barrier, inc=1, device_id=(e, (t + k) % tp_count), device_id_type=MESH
        )
    for copy in loads:
        copy.start()
    pl.semaphore_wait(barrier, ep_count - 1 + tp_count - 1)

    def wz(to, origin):
        return remote(
            ow_hbm.at[
                pl.ds(pl.multiple_of(e * share, share), share),
                pl.ds(pl.multiple_of(to * feat, feat), feat),
            ],
            wcols.at[origin, e],
            wz_s.at[to],
            wz_r.at[origin],
            (e, to),
        )

    for k in range(1, tp_count):
        wz((t + k) % tp_count, t).start()

    def stacked(ref):
        return jnp.concatenate(
            [ref[h : h + 1, c * CH : (c + 1) * CH] for h in range(heads) for c in range(chunks)],
            axis=0,
        )

    gates = gate_rows(stacked(ig_ref), stacked(fg_ref))
    summary(heads, chunks, k_ref, v_ref, gates, sums, e)

    def st(peer, origin):
        return remote(
            sums.at[origin], sums.at[origin], st_s.at[peer], st_r.at[origin], (peer, t)
        )

    for dy, dx in around:
        st(ep_peer(dy, dx), e).start()

    width = tiles(half, 512)
    square = jnp.zeros((count, 1), F32)
    for n in range(0, depth, width):
        wide = rows_ref[:, n : n + width].astype(F32)
        square = square + jnp.sum(wide * wide, axis=1, keepdims=True)
    inverse = lax.rsqrt(square / depth + 1e-06)
    for n in range(0, depth, width):
        wide = rows_ref[:, n : n + width].astype(F32)
        normed[:, n : n + width] = (wide * inverse * mg_ref[:, n : n + width]).astype(BF16)

    lane = lax.broadcasted_iota(jnp.int32, (count, 128), 1)
    topk = routes_ref.shape[1]
    named = [lane == routes_ref[:, k : k + 1] for k in range(topk)]
    member = named[0]
    for k in range(1, topk):
        member = member | named[k]
    earlier = lax.broadcasted_iota(jnp.int32, (count, count), 0) > lax.broadcasted_iota(
        jnp.int32, (count, count), 1
    )
    before = jnp.dot(
        jnp.where(earlier, 1.0, 0.0).astype(BF16),
        jnp.where(member, 1.0, 0.0).astype(BF16),
        preferred_element_type=F32,
    )
    slot_no = lax.broadcasted_iota(jnp.int32, (count, slots), 1)
    place = jnp.zeros((count, slots), F32)
    weight = jnp.zeros((count, slots), F32)
    for k in range(topk):
        ahead = jnp.sum(jnp.where(named[k], before, 0.0), axis=1, keepdims=True)
        target = routes_ref[:, k : k + 1] * cap + ahead.astype(jnp.int32)
        hit = slot_no == target
        place = jnp.where(hit, 1.0, place)
        weight = jnp.where(hit, rw_ref[:, k : k + 1], weight)
    place = place.astype(BF16)
    weight_high, weight_low = split_bf16(weight)

    def stage(side_no):
        for n in range(0, half, width):
            cols = pl.ds(pl.multiple_of(side_no * half + n, width), width)
            moved = lax.dot_general(
                place, normed[:, cols], (((0,), (0,)), ((), ())), preferred_element_type=F32
            ).astype(BF16)
            for x in range(ep_count):
                staged[side_no, x, :, n : n + width] = moved[x * cap : (x + 1) * cap]

    def dx_copy(peer, origin):
        return remote(
            staged.at[core, peer],
            arrived.at[core, origin],
            dx_s.at[peer],
            dx_r.at[origin],
            (peer, t),
        )

    def dp_copy(origin):
        return remote(
            arrived.at[core, origin],
            arrived.at[core, origin],
            dp_s.at[origin],
            dp_r.at[origin],
            (e, 2 * z + 1 - core),
        )

    def dp_other(origin):
        return remote(
            arrived.at[core, origin],
            arrived.at[1 - core, origin],
            dp_s.at[origin],
            dp_r.at[origin],
            (e, 2 * z + 1 - core),
        )

    stage(core)
    for dy, dx in around:
        dx_copy(ep_peer(dy, dx), e).start()
    stage(1 - core)
    for s in range(2):
        arrived[s, e] = staged[s, e]

    loads[0].wait()
    loads[1].wait()
    gate = jnp.dot(normed[...], sg[...], preferred_element_type=F32)
    up = jnp.dot(normed[...], su[...], preferred_element_type=F32)
    shared_hidden[...] = (gate / (1.0 + jnp.exp(-gate)) * up).astype(BF16)

    def line(kind, part, origin, where):
        sems = {"up": (up_s, up_r), "dn": (dn_s, dn_r), "pa": (pa_s, pa_r)}[kind]
        ref = mixed.at[2 * origin + core, pl.ds(part * seg, seg)]
        return remote(
            ref, ref, sems[0].at[part, origin], sems[1].at[part, origin], (e, where)
        )

    def line_other(part, origin):
        ref = mixed.at[2 * origin + 1 - core, pl.ds(part * seg, seg)]
        return remote(
            ref, ref, pa_s.at[part, origin], pa_r.at[part, origin], (e, 2 * z + 1 - core)
        )

    def go_up(part, origin):
        @pl.when(z + 1 < chips)
        def _():
            line("up", part, origin, t + 2).start()

    def go_down(part, origin):
        @pl.when(z > 0)
        def _():
            line("dn", part, origin, t - 2).start()

    def go_across(part, origin):
        line("pa", part, origin, 2 * z + 1 - core).start()

    def after(c):
        if (c + 1) % (chunks // SPLIT) == 0:
            part = (c + 1) // (chunks // SPLIT) - 1
            mixed[t, part * seg : (part + 1) * seg] = own[part * seg : (part + 1) * seg]
            go_up(part, z)
            go_down(part, z)
            go_across(part, z)

    def relay(step):
        for part in range(SPLIT):

            @pl.when(z >= step)
            def _():
                line("up", part, z - step, t - 2).wait_recv()
                go_up(part, z - step)
                go_across(part, z - step)

            @pl.when(z + step < chips)
            def _():
                line("dn", part, z + step, t + 2).wait_recv()
                go_down(part, z + step)
                go_across(part, z + step)

    for dy, dx in around:
        peer = ep_peer(dy, dx)
        st(peer, peer).wait_recv()
    state, stab = entering_state(heads, e, sums)
    cell_blocks(
        heads, chunks, state, stab, gates, q_ref, k_ref, v_ref, og_ref, gain_ref, own, after
    )

    def wx(part, peer, origin):
        ref = wcols.at[pl.ds(part * group, group), origin]
        return remote(ref, ref, wx_s.at[part, peer], wx_r.at[part, origin], (peer, t))

    loads[6].wait()
    for k in range(1, tp_count):
        wz((t + k) % tp_count, (t + k) % tp_count).wait_recv()
    for dy, dx in around:
        wx(0, ep_peer(dy, dx), e).start()

    for dy, dx in around:
        origin = ep_peer(dy, dx)
        dx_copy(origin, origin).wait_recv()
        dp_copy(origin).start()
    for dy, dx in around:
        dp_other(ep_peer(dy, dx)).wait_recv()

    loads[2].wait()
    loads[3].wait()
    units = eg.shape[1]
    tile = tiles(units, 256)

    def both(weights, n):
        return sum(
            jnp.dot(
                arrived[s].reshape(slots, half),
                weights[s * half : (s + 1) * half, n : n + tile],
                preferred_element_type=F32,
            )
            for s in range(2)
        )

    for n in range(0, units, tile):
        gate = both(eg, n)
        up = both(eu, n)
        hidden[:, n : n + tile] = (gate / (1.0 + jnp.exp(-gate)) * up).astype(BF16)
    relay(1)

    loads[4].wait()
    loads[5].wait()

    def pp(block):
        return remote(
            give.at[block], take.at[block], pp_s.at[block], pp_r.at[block],
            (e, 2 * z + 1 - core),
        )

    def products(block, owner):
        cols = pl.ds(pl.multiple_of((2 * block + owner) * feat, feat), feat)
        return (
            jnp.dot(hidden[...], ed[:, cols], preferred_element_type=F32),
            jnp.dot(shared_hidden[...], sd[:, cols], preferred_element_type=F32),
        )

    for block in range(chips):
        routed, common = products(block, 1 - core)
        give[block, 0:slots] = routed.astype(BF16)
        give[block, slots:] = common.astype(BF16)
        pp(block).start()
    for block in range(chips):
        routed, common = products(block, core)
        pp(block).wait_recv()
        total = (routed + take[block, 0:slots].astype(F32)).astype(BF16)
        for x in range(ep_count):
            reduced[block, x] = total[x * cap : (x + 1) * cap]
        shared_own[block] = common + take[block, slots:].astype(F32)

    def rt(peer, origin):
        return remote(
            reduced.at[:, peer], returned.at[:, origin], rt_s.at[peer], rt_r.at[origin], (peer, t)
        )

    for dy, dx in around:
        rt(ep_peer(dy, dx), e).start()
    for block in range(chips):
        returned[block, e] = reduced[block, e]
    for dy, dx in around:
        wx(1, ep_peer(dy, dx), e).start()
    for step in range(2, chips):
        relay(step)

    for dy, dx in around:
        origin = ep_peer(dy, dx)
        rt(origin, origin).wait_recv()

    def zs(to, origin):
        return remote(
            part_out.at[to], part_in.at[origin], zs_s.at[to], zs_r.at[origin], (e, 2 * to + core)
        )

    for block in range(chips):
        results = returned[block].reshape(slots, feat)
        total = (
            jnp.dot(weight_high, results, preferred_element_type=F32)
            + jnp.dot(weight_low, results, preferred_element_type=F32)
            + shared_own[block]
        )
        part_out[block] = total.astype(BF16)

        @pl.when(z == block)
        def _():
            final[...] = total

    for k in range(1, chips):
        zs((z + k) % chips, z).start()

    for part in range(SPLIT):
        for dy, dx in around:
            origin = ep_peer(dy, dx)
            wx(part, origin, origin).wait_recv()
    for part in range(SPLIT):
        for origin in range(chips):
            line_other(part, origin).wait_recv()
    step_rows = tiles(tok, 256)

    @pl.loop(0, tok // step_rows)
    def _(i):
        rows = pl.ds(pl.multiple_of(i * step_rows, step_rows), step_rows)
        total = 0.0
        for b in range(tp_count):
            total = total + jnp.dot(
                mixed[b, rows],
                wcols[b].reshape(ep_count * share, feat),
                preferred_element_type=F32,
            )
        mixer_out[rows, :] = total.astype(BF16)

    total = final[...]
    for k in range(1, chips):
        origin = (z + k) % chips
        zs(origin, origin).wait_recv()
        total = total + part_in[origin].astype(F32)
    moe_out[...] = total.astype(BF16)

    for k in range(1, tp_count):
        wz((t + k) % tp_count, t).wait_send()
    for dy, dx in around:
        peer = ep_peer(dy, dx)
        st(peer, e).wait_send()
        dx_copy(peer, e).wait_send()
        dp_copy(peer).wait_send()
        rt(peer, e).wait_send()
        for part in range(SPLIT):
            wx(part, peer, e).wait_send()
    for block in range(chips):
        pp(block).wait_send()
    for k in range(1, chips):
        zs((z + k) % chips, z).wait_send()
    for part in range(SPLIT):
        for origin in range(chips):
            line("pa", part, origin, 2 * z + 1 - core).wait_send()

            @pl.when((origin <= z) & (z + 1 < chips))
            def _():
                line("up", part, origin, t + 2).wait_send()

            @pl.when((origin >= z) & (z > 0))
            def _():
                line("dn", part, origin, t - 2).wait_send()


def local(
    queries,
    keys,
    values,
    out_gate,
    in_gate,
    forget_gate,
    out_gain,
    out_weight,
    moe_rows,
    moe_gain,
    routes,
    route_weight,
    expert_gate,
    expert_up,
    expert_down,
    shared_gate,
    shared_up,
    shared_down,
):
    tp_count = lax.axis_size("tp")
    ep_count = lax.axis_size("ep")
    count, depth = moe_rows.shape
    assert expert_gate.shape[0] == 1
    cap = 3 * count * routes.shape[1] // (2 * ep_count)
    slots = ep_count * cap
    heads = in_gate.shape[0]
    tok = queries.shape[0]
    held = heads * DK
    extra = -(-(1 + 2 * heads) // 8) * 8
    chips = tp_count // 2
    units, common = expert_gate.shape[2], shared_gate.shape[1]
    wide, features = out_weight.shape
    feat = features // tp_count
    share = wide // ep_count
    half = depth // 2
    side = 1
    while side * side < ep_count:
        side *= 2
    dma = pltpu.SemaphoreType.DMA

    def vm(*shape, dtype=BF16):
        return pltpu.VMEM(shape, dtype)

    scratch = [
        vm(ep_count, held + extra, 128, dtype=F32),
        vm(tok, heads * DV),
        vm(tp_count, tok, heads * DV),
        vm(tp_count, ep_count, share, feat),
        vm(count, depth),
        vm(2, ep_count, cap, half),
        vm(2, ep_count, cap, half),
        vm(depth, units),
        vm(depth, units),
        vm(units, depth),
        vm(depth, common),
        vm(depth, common),
        vm(common, depth),
        vm(slots, units),
        vm(count, common),
        vm(chips, slots + count, feat),
        vm(chips, slots + count, feat),
        vm(chips, ep_count, cap, feat),
        vm(chips, ep_count, cap, feat),
        vm(chips, count, feat, dtype=F32),
        vm(chips, count, feat),
        vm(chips, count, feat),
        vm(count, feat, dtype=F32),
        dma((7,)),
    ]
    scratch += [dma((tp_count,))] * 2
    scratch += [dma((SPLIT, ep_count))] * 2
    scratch += [dma((ep_count,))] * 6
    scratch += [dma((SPLIT, chips))] * 6
    scratch += [dma((chips,))] * 2
    scratch += [dma((ep_count,))] * 2
    scratch += [dma((chips,))] * 2
    return pl.pallas_call(
        functools.partial(step_kernel, ep_count, tp_count, side, cap),
        out_shape=(
            jax.ShapeDtypeStruct((tok, feat), BF16),
            jax.ShapeDtypeStruct((count, feat), BF16),
        ),
        in_specs=[VM] * 11 + [ANY] * 7,
        out_specs=(VM, VM),
        scratch_shapes=scratch,
        compiler_params=pltpu.CompilerParams(
            collective_id=0, has_side_effects=True, vmem_limit_bytes=60 * 1024 * 1024
        ),
        cost_estimate=pl.CostEstimate(
            flops=9_000_000_000, bytes_accessed=30_000_000, transcendentals=0
        ),
    )(
        queries,
        keys,
        values,
        out_gate,
        in_gate,
        forget_gate,
        out_gain.reshape(1, -1),
        moe_rows,
        moe_gain.reshape(1, -1),
        routes,
        route_weight,
        out_weight,
        expert_gate,
        expert_up,
        expert_down,
        shared_gate,
        shared_up,
        shared_down,
    )


def solution(mesh):
    return jax.shard_map(
        local,
        mesh=mesh,
        in_specs=(
            P("ep", "tp"),
            P("ep", "tp"),
            P("ep", "tp"),
            P("ep", "tp"),
            P("tp", "ep"),
            P("tp", "ep"),
            P("tp"),
            P("tp", None),
            P("ep", None),
            P(),
            P("ep", None),
            P("ep", None),
            P("ep", None, "tp"),
            P("ep", None, "tp"),
            P("ep", "tp", None),
            P(None, "tp"),
            P(None, "tp"),
            P("tp", None),
        ),
        out_specs=(P("ep", "tp"), P("ep", "tp")),
        check_vma=False,
    )
```

time: 215 us -> 84.8 us (0.39)
  waiting for transfers between devices: 85.2 us -> 0 us
  blocking collectives: 40.3 us -> 0 us
  Pallas kernels: 42.2 us -> 78.2 us
  between operations: 15.6 us -> 0.65 us
  starting transfers between devices: 8.93 us -> 0 us
  local copies, waits for them, and re-layouts: 12.5 us -> 5.78 us
  matrix products: 4.88 us -> 0 us
  other arithmetic: 3.61 us -> 0 us
    all_gather x2 -> x0, waiting for transfers between devices: 53.1 us -> none  [the longest x1 46.1 us: local(): gathered = lax.all_gather(mixed, 'tp')]
    pallas_call x6 -> x1, Pallas kernels: 42.2 us -> 78.2 us  [local(): pl.pallas_call(functools.partial(step_kernel, ep_count, tp_count, side, c...]
    all_to_all x2 -> x0, waiting for transfers between devices: 29.6 us -> none  [the longest x1 29.6 us: local(): lax.all_to_all(outgoing, 'ep', split_axis=0, concat_axis=0, tiled=True)]
    all_to_all x1 -> x0, blocking collectives: 29.1 us -> none  [weight_columns(): part = lax.all_to_all(part, 'tp', split_axis=0, concat_axis=0, tiled=True)]
    all_gather x1 -> x0, blocking collectives: 11.2 us -> none  [mixed_cells(): everything = lax.all_gather(summary, 'ep')]
    all_to_all x2 -> x0, starting transfers between devices: 8.84 us -> none  [the longest x1 5.19 us: local(): lax.all_to_all(outgoing, 'ep', split_axis=0, concat_axis=0, tiled=True)]
    dot_general x3 -> x0, matrix products: 4.88 us -> none  [the longest x1 2.67 us: local(): lax.dot_general(place, normed, (((0,), (0,)), ((), ())), preferred_elemen...]
    reshape x3 -> x0, local copies, waits for them, and re-layouts: 4.35 us -> none  [the longest x1 3.14 us: weight_columns(): return whole.transpose(1, 0, 2).reshape(tp_count * depth, mine)]
  transfers between devices with their start and end apart: 5 -> 0, of which waited for: 4 -> 0; matrix products, arithmetic and copies ran while one was open for 5% -> 0% of each run, Pallas kernels for 11% -> 0%
where the time goes in v1:
time: 84.8 us; the launch traced here: 84.6 us
  Pallas kernels  78.2 us (92%)
  local copies, waits for them, and re-layouts  5.78 us (7%)
    pallas_call x1, Pallas kernels, local(): pl.pallas_call(functools.partial(step_kernel, ep_count, tp_count, side, c...  78.2 us
    unnamed x6, local copies, waits for them, and re-layouts  5.78 us

profile of v1, /device:TPU:0, one launch (start us, length us, event | category | flops | bytes accessed | tf_op | source)
XLA Modules:
  0.0 84.6 jit_solution(3361338362453630517)
XLA Ops:
  0.6 1.4 %copy.20.routes_ref = s32[128,2]{1,0:T(8,128)} copy(s32[128,2]{0,1:T(2,128)} %param.28) | data formatting | bytes 2048 | tf_op args[10]
  2.0 1.4 %copy.21.rw_ref = f32[128,2]{1,0:T(8,128)} copy(f32[128,2]{0,1:T(2,128)} %param.29) | data formatting | bytes 2048 | tf_op args[11]
  3.5 78.2 %shard_map.185 = (bf16[1024,512]{1,0:T(8,128)(2,1)}, bf16[128,512]{1,0:T(8,128)(2,1)}) custom-call(bf16[1024,128]{1,0:T(8,128)(2,1)} %q_ref.1, bf16[1024,128]{1,0:T(8,128)(2,1)} %k_ref.1, bf16[1024,256]{1,0:T(8,128)(2,1)} %v_ref.1, bf16[1024,256]{1,0:T(8,128)(2,1)} %og_ref.1, f32[2,1024]{1,0:T(2,128)} %ig_ref.1, f32[2,1024]{1,0:T(2,128)} %fg_ref.1, ...), custom_call_target="tpu_custom_call" | custom-call | flops 8999999488 | bytes 30000000 | tf_op jit(solution)/shard_map/pallas_call | solution.py:765
  81.7 0.0 copy-start
  81.7 2.3 %copy.24 = bf16[1024,512]{1,0:T(8,128)(2,1)} copy(bf16[1024,512]{1,0:T(8,128)(2,1)} %get-tuple-element.4) | data formatting | bytes 2097152
  84.0 0.0 copy-done
  84.0 0.7 copy.25
Async XLA Ops:
  81.7 2.3 %copy-start = (bf16[128,512]{1,0:T(8,128)(2,1)S(1)}, bf16[128,512]{1,0:T(8,128)(2,1)}, u32[]{:S(2)}) copy-start(bf16[128,512]{1,0:T(8,128)(2,1)} %get-tuple-element.5) | copy-start | bytes 393220

commit v2 on v1

--- a/solution.py
+++ b/solution.py
@@ -225,17 +225,17 @@
     tp_count,
     side,
     cap,
-    q_ref,
-    k_ref,
-    v_ref,
-    og_ref,
     ig_ref,
     fg_ref,
     gain_ref,
-    rows_ref,
     mg_ref,
     routes_ref,
     rw_ref,
+    q_hbm,
+    k_hbm,
+    v_hbm,
+    og_hbm,
+    rows_hbm,
     ow_hbm,
     eg_hbm,
     eu_hbm,
@@ -249,6 +249,12 @@
     own,
     mixed,
     wcols,
+    out_rows,
+    tokens,
+    q_ref,
+    k_ref,
+    v_ref,
+    og_ref,
     normed,
     staged,
     arrived,
@@ -269,10 +275,12 @@
     part_in,
     final,
     load_sem,
+    out_sem,
     wz_s,
     wz_r,
     wx_s,
     wx_r,
+    wf_s,
     st_s,
     st_r,
     dx_s,
@@ -298,12 +306,13 @@
     heads = ig_ref.shape[0]
     tok = q_ref.shape[0]
     chunks = tok // CH
-    count, depth = rows_ref.shape
+    count, depth = tokens.shape
     half = depth // 2
     feat = mixer_out.shape[1]
     share = wcols.shape[2]
     slots = ep_count * cap
     group = tp_count // SPLIT
+    batch = chips // SPLIT
     seg = tok // SPLIT
 
     def ep_peer(dy, dx):
@@ -319,26 +328,6 @@
             device_id_type=MESH,
         )
 
-    loads = [
-        pltpu.make_async_copy(src, dst, load_sem.at[i])
-        for i, (src, dst) in enumerate(
-            [
-                (sg_hbm, sg),
-                (su_hbm, su),
-                (eg_hbm.at[0], eg),
-                (eu_hbm.at[0], eu),
-                (ed_hbm.at[0], ed),
-                (sd_hbm, sd),
-                (
-                    ow_hbm.at[
-                        pl.ds(pl.multiple_of(e * share, share), share),
-                        pl.ds(pl.multiple_of(t * feat, feat), feat),
-                    ],
-                    wcols.at[t, e],
-                ),
-            ]
-        )
-    ]
     barrier = pltpu.get_barrier_semaphore()
     for dy, dx in around:
         pl.semaphore_signal(barrier, inc=1, device_id=(ep_peer(dy, dx), t), device_id_type=MESH)
@@ -346,8 +335,30 @@
         pl.semaphore_signal(
             barrier, inc=1, device_id=(e, (t + k) % tp_count), device_id_type=MESH
         )
-    for copy in loads:
-        copy.start()
+    loads = {}
+    for name, src, dst in (
+        ("k", k_hbm, k_ref),
+        ("v", v_hbm, v_ref),
+        ("tokens", rows_hbm, tokens),
+        ("sg", sg_hbm, sg),
+        ("su", su_hbm, su),
+        ("q", q_hbm, q_ref),
+        ("og", og_hbm, og_ref),
+        (
+            "own",
+            ow_hbm.at[
+                pl.ds(pl.multiple_of(e * share, share), share),
+                pl.ds(pl.multiple_of(t * feat, feat), feat),
+            ],
+            wcols.at[t, e],
+        ),
+        ("eg", eg_hbm.at[0], eg),
+        ("eu", eu_hbm.at[0], eu),
+        ("ed", ed_hbm.at[0], ed),
+        ("sd", sd_hbm, sd),
+    ):
+        loads[name] = pltpu.make_async_copy(src, dst, load_sem.at[len(loads)])
+        loads[name].start()
     pl.semaphore_wait(barrier, ep_count - 1 + tp_count - 1)
 
     def wz(to, origin):
@@ -372,6 +383,8 @@
         )
 
     gates = gate_rows(stacked(ig_ref), stacked(fg_ref))
+    loads["k"].wait()
+    loads["v"].wait()
     summary(heads, chunks, k_ref, v_ref, gates, sums, e)
 
     def st(peer, origin):
@@ -382,19 +395,21 @@
     for dy, dx in around:
         st(ep_peer(dy, dx), e).start()
 
+    loads["tokens"].wait()
     width = tiles(half, 512)
     square = jnp.zeros((count, 1), F32)
     for n in range(0, depth, width):
-        wide = rows_ref[:, n : n + width].astype(F32)
+        wide = tokens[:, n : n + width].astype(F32)
         square = square + jnp.sum(wide * wide, axis=1, keepdims=True)
     inverse = lax.rsqrt(square / depth + 1e-06)
     for n in range(0, depth, width):
-        wide = rows_ref[:, n : n + width].astype(F32)
+        wide = tokens[:, n : n + width].astype(F32)
         normed[:, n : n + width] = (wide * inverse * mg_ref[:, n : n + width]).astype(BF16)
 
-    lane = lax.broadcasted_iota(jnp.int32, (count, 128), 1)
-    topk = routes_ref.shape[1]
-    named = [lane == routes_ref[:, k : k + 1] for k in range(topk)]
+    topk = routes_ref.shape[0]
+    table = columns_of([routes_ref[...].astype(F32), rw_ref[...]])
+    lane = lax.broadcasted_iota(jnp.int32, (count, 128), 1).astype(F32)
+    named = [lane == table[:, k : k + 1] for k in range(topk)]
     member = named[0]
     for k in range(1, topk):
         member = member | named[k]
@@ -406,15 +421,14 @@
         jnp.where(member, 1.0, 0.0).astype(BF16),
         preferred_element_type=F32,
     )
-    slot_no = lax.broadcasted_iota(jnp.int32, (count, slots), 1)
+    slot_no = lax.broadcasted_iota(jnp.int32, (count, slots), 1).astype(F32)
     place = jnp.zeros((count, slots), F32)
     weight = jnp.zeros((count, slots), F32)
     for k in range(topk):
         ahead = jnp.sum(jnp.where(named[k], before, 0.0), axis=1, keepdims=True)
-        target = routes_ref[:, k : k + 1] * cap + ahead.astype(jnp.int32)
-        hit = slot_no == target
+        hit = slot_no == table[:, k : k + 1] * cap + ahead
         place = jnp.where(hit, 1.0, place)
-        weight = jnp.where(hit, rw_ref[:, k : k + 1], weight)
+        weight = jnp.where(hit, table[:, topk + k : topk + k + 1], weight)
     place = place.astype(BF16)
     weight_high, weight_low = split_bf16(weight)
 
@@ -455,14 +469,12 @@
         )
 
     stage(core)
-    for dy, dx in around:
-        dx_copy(ep_peer(dy, dx), e).start()
     stage(1 - core)
     for s in range(2):
         arrived[s, e] = staged[s, e]
 
-    loads[0].wait()
-    loads[1].wait()
+    loads["sg"].wait()
+    loads["su"].wait()
     gate = jnp.dot(normed[...], sg[...], preferred_element_type=F32)
     up = jnp.dot(normed[...], su[...], preferred_element_type=F32)
     shared_hidden[...] = (gate / (1.0 + jnp.exp(-gate)) * up).astype(BF16)
@@ -501,48 +513,64 @@
             go_down(part, z)
             go_across(part, z)
 
-    def relay(step):
-        for part in range(SPLIT):
-
-            @pl.when(z >= step)
-            def _():
-                line("up", part, z - step, t - 2).wait_recv()
-                go_up(part, z - step)
-                go_across(part, z - step)
-
-            @pl.when(z + step < chips)
-            def _():
-                line("dn", part, z + step, t + 2).wait_recv()
-                go_down(part, z + step)
-                go_across(part, z + step)
+    def relay(step, part):
+        if step >= chips:
+            return
+
+        @pl.when(z >= step)
+        def _():
+            line("up", part, z - step, t - 2).wait_recv()
+            go_up(part, z - step)
+            go_across(part, z - step)
+
+        @pl.when(z + step < chips)
+        def _():
+            line("dn", part, z + step, t + 2).wait_recv()
+            go_down(part, z + step)
+            go_across(part, z + step)
 
     for dy, dx in around:
         peer = ep_peer(dy, dx)
         st(peer, peer).wait_recv()
+    for dy, dx in around:
+        dx_copy(ep_peer(dy, dx), e).start()
+    loads["q"].wait()
+    loads["og"].wait()
     state, stab = entering_state(heads, e, sums)
     cell_blocks(
         heads, chunks, state, stab, gates, q_ref, k_ref, v_ref, og_ref, gain_ref, own, after
     )
 
+    rowwise = [(dy, dx) for dy, dx in around if dy == 0]
+    columnwise = [(dy, dx) for dy, dx in around if dx == 0]
+
     def wx(part, peer, origin):
         ref = wcols.at[pl.ds(part * group, group), origin]
         return remote(ref, ref, wx_s.at[part, peer], wx_r.at[part, origin], (peer, t))
 
-    loads[6].wait()
-    for k in range(1, tp_count):
-        wz((t + k) % tp_count, (t + k) % tp_count).wait_recv()
-    for dy, dx in around:
-        wx(0, ep_peer(dy, dx), e).start()
-
+    def wf(part, peer, origin):
+        ref = wcols.at[pl.ds(part * group, group), origin]
+        return remote(ref, ref, wf_s.at[origin, peer], wx_r.at[part, origin], (peer, t))
+
+    paths = ((rowwise, columnwise), (columnwise, rowwise))
+
+    relay(1, 0)
     for dy, dx in around:
         origin = ep_peer(dy, dx)
         dx_copy(origin, origin).wait_recv()
         dp_copy(origin).start()
+    loads["own"].wait()
+    for k in range(1, tp_count):
+        wz((t + k) % tp_count, (t + k) % tp_count).wait_recv()
+    for part in range(SPLIT):
+        for dy, dx in rowwise + columnwise:
+            wx(part, ep_peer(dy, dx), e).start()
+    relay(1, 1)
     for dy, dx in around:
         dp_other(ep_peer(dy, dx)).wait_recv()
 
-    loads[2].wait()
-    loads[3].wait()
+    loads["eg"].wait()
+    loads["eu"].wait()
     units = eg.shape[1]
     tile = tiles(units, 256)
 
@@ -560,10 +588,9 @@
         gate = both(eg, n)
         up = both(eu, n)
         hidden[:, n : n + tile] = (gate / (1.0 + jnp.exp(-gate)) * up).astype(BF16)
-    relay(1)
-
-    loads[4].wait()
-    loads[5].wait()
+
+    loads["ed"].wait()
+    loads["sd"].wait()
 
     def pp(block):
         return remote(
@@ -583,6 +610,18 @@
         give[block, 0:slots] = routed.astype(BF16)
         give[block, slots:] = common.astype(BF16)
         pp(block).start()
+    relay(2, 0)
+
+    def rt(part, peer, origin):
+        blocks = pl.ds(part * batch, batch)
+        return remote(
+            reduced.at[blocks, peer],
+            returned.at[blocks, origin],
+            rt_s.at[part, peer],
+            rt_r.at[part, origin],
+            (peer, t),
+        )
+
     for block in range(chips):
         routed, common = products(block, core)
         pp(block).wait_recv()
@@ -590,50 +629,57 @@
         for x in range(ep_count):
             reduced[block, x] = total[x * cap : (x + 1) * cap]
         shared_own[block] = common + take[block, slots:].astype(F32)
-
-    def rt(peer, origin):
-        return remote(
-            reduced.at[:, peer], returned.at[:, origin], rt_s.at[peer], rt_r.at[origin], (peer, t)
-        )
-
-    for dy, dx in around:
-        rt(ep_peer(dy, dx), e).start()
+        if (block + 1) % batch == 0:
+            for dy, dx in around:
+                rt(block // batch, ep_peer(dy, dx), e).start()
     for block in range(chips):
         returned[block, e] = reduced[block, e]
-    for dy, dx in around:
-        wx(1, ep_peer(dy, dx), e).start()
-    for step in range(2, chips):
-        relay(step)
-
-    for dy, dx in around:
-        origin = ep_peer(dy, dx)
-        rt(origin, origin).wait_recv()
+    relay(2, 1)
+    for part, (near, far) in enumerate(paths):
+        for dy, dx in near:
+            origin = ep_peer(dy, dx)
+            wx(part, origin, origin).wait_recv()
+            for fy, fx in far:
+                wf(part, ep_peer(fy, fx), origin).start()
 
     def zs(to, origin):
         return remote(
             part_out.at[to], part_in.at[origin], zs_s.at[to], zs_r.at[origin], (e, 2 * to + core)
         )
-
-    for block in range(chips):
-        results = returned[block].reshape(slots, feat)
-        total = (
-            jnp.dot(weight_high, results, preferred_element_type=F32)
-            + jnp.dot(weight_low, results, preferred_element_type=F32)
-            + shared_own[block]
-        )
-        part_out[block] = total.astype(BF16)
-
-        @pl.when(z == block)
-        def _():
-            final[...] = total
-
-    for k in range(1, chips):
-        zs((z + k) % chips, z).start()
 
     for part in range(SPLIT):
         for dy, dx in around:
             origin = ep_peer(dy, dx)
-            wx(part, origin, origin).wait_recv()
+            rt(part, origin, origin).wait_recv()
+        for block in range(part * batch, (part + 1) * batch):
+            results = returned[block].reshape(slots, feat)
+            total = (
+                jnp.dot(weight_high, results, preferred_element_type=F32)
+                + jnp.dot(weight_low, results, preferred_element_type=F32)
+                + shared_own[block]
+            )
+            part_out[block] = total.astype(BF16)
+
+            @pl.when(z == block)
+            def _():
+                final[...] = total
+
+            @pl.when(z != block)
+            def _():
+                zs(block, z).start()
+
+        for step in range(3, chips):
+            relay(step, part)
+
+    for dy, dx in around:
+        origin = ep_peer(dy, dx)
+        if dy == 0:
+            wx(1, origin, origin).wait_recv()
+        elif dx == 0:
+            wx(0, origin, origin).wait_recv()
+        else:
+            for part in range(SPLIT):
+                wx(part, origin, origin).wait_recv()
     for part in range(SPLIT):
         for origin in range(chips):
             line_other(part, origin).wait_recv()
@@ -649,7 +695,8 @@
                 wcols[b].reshape(ep_count * share, feat),
                 preferred_element_type=F32,
             )
-        mixer_out[rows, :] = total.astype(BF16)
+        out_rows[rows] = total.astype(BF16)
+        pltpu.make_async_copy(out_rows.at[rows], mixer_out.at[rows], out_sem.at[i]).start()
 
     total = final[...]
     for k in range(1, chips):
@@ -660,18 +707,28 @@
 
     for k in range(1, tp_count):
         wz((t + k) % tp_count, t).wait_send()
+    for dy, dx in rowwise + columnwise:
+        for part in range(SPLIT):
+            wx(part, ep_peer(dy, dx), e).wait_send()
+    for part, (near, far) in enumerate(paths):
+        for dy, dx in near:
+            for fy, fx in far:
+                wf(part, ep_peer(fy, fx), ep_peer(dy, dx)).wait_send()
     for dy, dx in around:
         peer = ep_peer(dy, dx)
         st(peer, e).wait_send()
         dx_copy(peer, e).wait_send()
         dp_copy(peer).wait_send()
-        rt(peer, e).wait_send()
         for part in range(SPLIT):
-            wx(part, peer, e).wait_send()
+            rt(part, peer, e).wait_send()
     for block in range(chips):
         pp(block).wait_send()
-    for k in range(1, chips):
-        zs((z + k) % chips, z).wait_send()
+    for block in range(chips):
+
+        @pl.when(z != block)
+        def _():
+            zs(block, z).wait_send()
+
     for part in range(SPLIT):
         for origin in range(chips):
             line("pa", part, origin, 2 * z + 1 - core).wait_send()
@@ -683,6 +740,11 @@
             @pl.when((origin >= z) & (z > 0))
             def _():
                 line("dn", part, origin, t - 2).wait_send()
+
+    @pl.loop(0, tok // step_rows)
+    def _(i):
+        rows = pl.ds(pl.multiple_of(i * step_rows, step_rows), step_rows)
+        pltpu.make_async_copy(out_rows.at[rows], mixer_out.at[rows], out_sem.at[i]).wait()
 
 
 def local(
@@ -734,6 +796,12 @@
         vm(tok, heads * DV),
         vm(tp_count, tok, heads * DV),
         vm(tp_count, ep_count, share, feat),
+        vm(tok, feat),
+        vm(count, depth),
+        vm(tok, held),
+        vm(tok, held),
+        vm(tok, heads * DV),
+        vm(tok, heads * DV),
         vm(count, depth),
         vm(2, ep_count, cap, half),
         vm(2, ep_count, cap, half),
@@ -753,14 +821,16 @@
         vm(chips, count, feat),
         vm(chips, count, feat),
         vm(count, feat, dtype=F32),
-        dma((7,)),
+        dma((12,)),
+        dma((-(-tok // 256),)),
     ]
     scratch += [dma((tp_count,))] * 2
     scratch += [dma((SPLIT, ep_count))] * 2
+    scratch += [dma((ep_count, ep_count))]
     scratch += [dma((ep_count,))] * 6
     scratch += [dma((SPLIT, chips))] * 6
     scratch += [dma((chips,))] * 2
-    scratch += [dma((ep_count,))] * 2
+    scratch += [dma((SPLIT, ep_count))] * 2
     scratch += [dma((chips,))] * 2
     return pl.pallas_call(
         functools.partial(step_kernel, ep_count, tp_count, side, cap),
@@ -768,8 +838,8 @@
             jax.ShapeDtypeStruct((tok, feat), BF16),
             jax.ShapeDtypeStruct((count, feat), BF16),
         ),
-        in_specs=[VM] * 11 + [ANY] * 7,
-        out_specs=(VM, VM),
+        in_specs=[VM] * 6 + [ANY] * 12,
+        out_specs=(ANY, VM),
         scratch_shapes=scratch,
         compiler_params=pltpu.CompilerParams(
             collective_id=0, has_side_effects=True, vmem_limit_bytes=60 * 1024 * 1024
@@ -778,17 +848,17 @@
             flops=9_000_000_000, bytes_accessed=30_000_000, transcendentals=0
         ),
     )(
+        in_gate,
+        forget_gate,
+        out_gain.reshape(1, -1),
+        moe_gain.reshape(1, -1),
+        routes.T,
+        route_weight.T,
         queries,
         keys,
         values,
         out_gate,
-        in_gate,
-        forget_gate,
-        out_gain.reshape(1, -1),
         moe_rows,
-        moe_gain.reshape(1, -1),
-        routes,
-        route_weight,
         out_weight,
         expert_gate,
         expert_up,

time: 84.8 us -> 77.8 us (0.917)
  Pallas kernels: 78.2 us -> 73.4 us
  local copies, waits for them, and re-layouts: 5.78 us -> 2.96 us
    pallas_call x1, Pallas kernels: 78.2 us -> 73.4 us  [local(): pl.pallas_call(functools.partial(step_kernel, ep_count, tp_count, side, c...]
    unnamed x6 -> x4, local copies, waits for them, and re-layouts: 5.78 us -> 2.96 us
where the time goes in v2:
time: 77.8 us; the launch traced here: 77.1 us
  Pallas kernels  73.4 us (94%)
  local copies, waits for them, and re-layouts  2.96 us (4%)
    pallas_call x1, Pallas kernels, local(): pl.pallas_call(functools.partial(step_kernel, ep_count, tp_count, side, c...  73.4 us
    unnamed x4, local copies, waits for them, and re-layouts  2.96 us

profile of v2, /device:TPU:0, one launch (start us, length us, event | category | flops | bytes accessed | tf_op | source)
XLA Modules:
  0.0 77.1 jit_solution(4811539187964460531)
XLA Ops:
  0.6 73.4 %shard_map.185 = (bf16[1024,512]{1,0:T(8,128)(2,1)}, bf16[128,512]{1,0:T(8,128)(2,1)}) custom-call(f32[2,1024]{1,0:T(2,128)} %ig_ref.1, f32[2,1024]{1,0:T(2,128)} %fg_ref.1, f32[1,256]{1,0:T(1,128)} %bitcast.5, f32[1,4096]{1,0:T(1,128)} %bitcast.4, s32[2,128]{1,0:T(2,128)} %bitcast.6, f32[2,128]{1,0:T(2,128)} %bitcast.7, bf16[1024,128]{1,0:T(8,128)(2,1)} %q_hbm.1, ...), custom_call_target="tpu_custom_call" | custom-call | flops 8999999488 | bytes 30000000 | tf_op jit(solution)/shard_map/pallas_call | solution.py:835
  74.1 0.0 copy-start
  74.1 2.3 %copy.22 = bf16[1024,512]{1,0:T(8,128)(2,1)} copy(bf16[1024,512]{1,0:T(8,128)(2,1)} %get-tuple-element.4) | data formatting | bytes 2097152
  76.4 0.0 copy-done
  76.4 0.7 copy.23
Async XLA Ops:
  74.1 2.3 %copy-start = (bf16[128,512]{1,0:T(8,128)(2,1)S(1)}, bf16[128,512]{1,0:T(8,128)(2,1)}, u32[]{:S(2)}) copy-start(bf16[128,512]{1,0:T(8,128)(2,1)} %get-tuple-element.5) | copy-start | bytes 393220

commit v3 on v2

--- a/solution.py
+++ b/solution.py
@@ -274,6 +274,7 @@
     part_out,
     part_in,
     final,
+    own_rows,
     load_sem,
     out_sem,
     wz_s,
@@ -313,6 +314,7 @@
     slots = ep_count * cap
     group = tp_count // SPLIT
     batch = chips // SPLIT
+    order = [b for i in range(chips // 2) for b in (i, chips - 1 - i)]
     seg = tok // SPLIT
 
     def ep_peer(dy, dx):
@@ -337,9 +339,9 @@
         )
     loads = {}
     for name, src, dst in (
+        ("tokens", rows_hbm, tokens),
         ("k", k_hbm, k_ref),
         ("v", v_hbm, v_ref),
-        ("tokens", rows_hbm, tokens),
         ("sg", sg_hbm, sg),
         ("su", su_hbm, su),
         ("q", q_hbm, q_ref),
@@ -375,25 +377,6 @@
 
     for k in range(1, tp_count):
         wz((t + k) % tp_count, t).start()
-
-    def stacked(ref):
-        return jnp.concatenate(
-            [ref[h : h + 1, c * CH : (c + 1) * CH] for h in range(heads) for c in range(chunks)],
-            axis=0,
-        )
-
-    gates = gate_rows(stacked(ig_ref), stacked(fg_ref))
-    loads["k"].wait()
-    loads["v"].wait()
-    summary(heads, chunks, k_ref, v_ref, gates, sums, e)
-
-    def st(peer, origin):
-        return remote(
-            sums.at[origin], sums.at[origin], st_s.at[peer], st_r.at[origin], (peer, t)
-        )
-
-    for dy, dx in around:
-        st(ep_peer(dy, dx), e).start()
 
     loads["tokens"].wait()
     width = tiles(half, 512)
@@ -441,12 +424,18 @@
             for x in range(ep_count):
                 staged[side_no, x, :, n : n + width] = moved[x * cap : (x + 1) * cap]
 
-    def dx_copy(peer, origin):
+    quarter = half // 2
+    early = [(0, dy, dx) for dy, dx in around[:1]]
+    middle = [(1, dy, dx) for dy, dx in around[:1]]
+    late = [(h, dy, dx) for dy, dx in around[1:] for h in range(2)]
+
+    def dx_copy(half_no, peer, origin):
+        cols = pl.ds(half_no * quarter, quarter)
         return remote(
-            staged.at[core, peer],
-            arrived.at[core, origin],
-            dx_s.at[peer],
-            dx_r.at[origin],
+            staged.at[core, peer, :, cols],
+            arrived.at[core, origin, :, cols],
+            dx_s.at[half_no, peer],
+            dx_r.at[half_no, origin],
             (peer, t),
         )
 
@@ -469,6 +458,28 @@
         )
 
     stage(core)
+    for half_no, dy, dx in early:
+        dx_copy(half_no, ep_peer(dy, dx), e).start()
+
+    def stacked(ref):
+        return jnp.concatenate(
+            [ref[h : h + 1, c * CH : (c + 1) * CH] for h in range(heads) for c in range(chunks)],
+            axis=0,
+        )
+
+    gates = gate_rows(stacked(ig_ref), stacked(fg_ref))
+    loads["k"].wait()
+    loads["v"].wait()
+    summary(heads, chunks, k_ref, v_ref, gates, sums, e)
+
+    def st(peer, origin):
+        return remote(
+            sums.at[origin], sums.at[origin], st_s.at[peer], st_r.at[origin], (peer, t)
+        )
+
+    for dy, dx in around:
+        st(ep_peer(dy, dx), e).start()
+
     stage(1 - core)
     for s in range(2):
         arrived[s, e] = staged[s, e]
@@ -478,6 +489,9 @@
     gate = jnp.dot(normed[...], sg[...], preferred_element_type=F32)
     up = jnp.dot(normed[...], su[...], preferred_element_type=F32)
     shared_hidden[...] = (gate / (1.0 + jnp.exp(-gate)) * up).astype(BF16)
+
+    for half_no, dy, dx in middle:
+        dx_copy(half_no, ep_peer(dy, dx), e).start()
 
     def line(kind, part, origin, where):
         sems = {"up": (up_s, up_r), "dn": (dn_s, dn_r), "pa": (pa_s, pa_r)}[kind]
@@ -532,8 +546,8 @@
     for dy, dx in around:
         peer = ep_peer(dy, dx)
         st(peer, peer).wait_recv()
-    for dy, dx in around:
-        dx_copy(ep_peer(dy, dx), e).start()
+    for half_no, dy, dx in late:
+        dx_copy(half_no, ep_peer(dy, dx), e).start()
     loads["q"].wait()
     loads["og"].wait()
     state, stab = entering_state(heads, e, sums)
@@ -554,16 +568,20 @@
 
     paths = ((rowwise, columnwise), (columnwise, rowwise))
 
+    loads["own"].wait()
+    for k in range(1, tp_count):
+        wz((t + k) % tp_count, (t + k) % tp_count).wait_recv()
+    for part, (near, far) in enumerate(paths):
+        for dy, dx in near:
+            wx(part, ep_peer(dy, dx), e).start()
     relay(1, 0)
     for dy, dx in around:
         origin = ep_peer(dy, dx)
-        dx_copy(origin, origin).wait_recv()
+        for half_no in range(2):
+            dx_copy(half_no, origin, origin).wait_recv()
         dp_copy(origin).start()
-    loads["own"].wait()
-    for k in range(1, tp_count):
-        wz((t + k) % tp_count, (t + k) % tp_count).wait_recv()
-    for part in range(SPLIT):
-        for dy, dx in rowwise + columnwise:
+    for part, (near, far) in enumerate(paths):
+        for dy, dx in far:
             wx(part, ep_peer(dy, dx), e).start()
     relay(1, 1)
     for dy, dx in around:
@@ -598,8 +616,8 @@
             (e, 2 * z + 1 - core),
         )
 
-    def products(block, owner):
-        cols = pl.ds(pl.multiple_of((2 * block + owner) * feat, feat), feat)
+    def products(place_no, owner):
+        cols = pl.ds(pl.multiple_of((2 * order[place_no] + owner) * feat, feat), feat)
         return (
             jnp.dot(hidden[...], ed[:, cols], preferred_element_type=F32),
             jnp.dot(shared_hidden[...], sd[:, cols], preferred_element_type=F32),
@@ -651,12 +669,13 @@
         for dy, dx in around:
             origin = ep_peer(dy, dx)
             rt(part, origin, origin).wait_recv()
-        for block in range(part * batch, (part + 1) * batch):
-            results = returned[block].reshape(slots, feat)
+        for place_no in range(part * batch, (part + 1) * batch):
+            block = order[place_no]
+            results = returned[place_no].reshape(slots, feat)
             total = (
                 jnp.dot(weight_high, results, preferred_element_type=F32)
                 + jnp.dot(weight_low, results, preferred_element_type=F32)
-                + shared_own[block]
+                + shared_own[place_no]
             )
             part_out[block] = total.astype(BF16)
 
@@ -670,6 +689,33 @@
 
         for step in range(3, chips):
             relay(step, part)
+
+    for k in range(1, tp_count):
+        wz((t + k) % tp_count, t).wait_send()
+    for dy, dx in rowwise + columnwise:
+        for part in range(SPLIT):
+            wx(part, ep_peer(dy, dx), e).wait_send()
+    for dy, dx in around:
+        peer = ep_peer(dy, dx)
+        st(peer, e).wait_send()
+        for half_no in range(2):
+            dx_copy(half_no, peer, e).wait_send()
+        dp_copy(peer).wait_send()
+        for part in range(SPLIT):
+            rt(part, peer, e).wait_send()
+    for block in range(chips):
+        pp(block).wait_send()
+    for part in range(SPLIT):
+        for origin in range(chips):
+            line("pa", part, origin, 2 * z + 1 - core).wait_send()
+
+            @pl.when((origin <= z) & (z + 1 < chips))
+            def _():
+                line("up", part, origin, t + 2).wait_send()
+
+            @pl.when((origin >= z) & (z > 0))
+            def _():
+                line("dn", part, origin, t - 2).wait_send()
 
     for dy, dx in around:
         origin = ep_peer(dy, dx)
@@ -695,7 +741,7 @@
                 wcols[b].reshape(ep_count * share, feat),
                 preferred_element_type=F32,
             )
-        out_rows[rows] = total.astype(BF16)
+        out_rows[rows] = total
         pltpu.make_async_copy(out_rows.at[rows], mixer_out.at[rows], out_sem.at[i]).start()
 
     total = final[...]
@@ -703,48 +749,26 @@
         origin = (z + k) % chips
         zs(origin, origin).wait_recv()
         total = total + part_in[origin].astype(F32)
-    moe_out[...] = total.astype(BF16)
-
-    for k in range(1, tp_count):
-        wz((t + k) % tp_count, t).wait_send()
-    for dy, dx in rowwise + columnwise:
-        for part in range(SPLIT):
-            wx(part, ep_peer(dy, dx), e).wait_send()
+    own_rows[...] = total
+    own_copy = pltpu.make_async_copy(own_rows, moe_out, load_sem.at[len(loads)])
+    own_copy.start()
+
     for part, (near, far) in enumerate(paths):
         for dy, dx in near:
             for fy, fx in far:
                 wf(part, ep_peer(fy, fx), ep_peer(dy, dx)).wait_send()
-    for dy, dx in around:
-        peer = ep_peer(dy, dx)
-        st(peer, e).wait_send()
-        dx_copy(peer, e).wait_send()
-        dp_copy(peer).wait_send()
-        for part in range(SPLIT):
-            rt(part, peer, e).wait_send()
-    for block in range(chips):
-        pp(block).wait_send()
     for block in range(chips):
 
         @pl.when(z != block)
         def _():
             zs(block, z).wait_send()
-
-    for part in range(SPLIT):
-        for origin in range(chips):
-            line("pa", part, origin, 2 * z + 1 - core).wait_send()
-
-            @pl.when((origin <= z) & (z + 1 < chips))
-            def _():
-                line("up", part, origin, t + 2).wait_send()
-
-            @pl.when((origin >= z) & (z > 0))
-            def _():
-                line("dn", part, origin, t - 2).wait_send()
 
     @pl.loop(0, tok // step_rows)
     def _(i):
         rows = pl.ds(pl.multiple_of(i * step_rows, step_rows), step_rows)
         pltpu.make_async_copy(out_rows.at[rows], mixer_out.at[rows], out_sem.at[i]).wait()
+
+    own_copy.wait()
 
 
 def local(
@@ -796,7 +820,7 @@
         vm(tok, heads * DV),
         vm(tp_count, tok, heads * DV),
         vm(tp_count, ep_count, share, feat),
-        vm(tok, feat),
+        vm(tok, feat, dtype=F32),
         vm(count, depth),
         vm(tok, held),
         vm(tok, held),
@@ -821,25 +845,28 @@
         vm(chips, count, feat),
         vm(chips, count, feat),
         vm(count, feat, dtype=F32),
-        dma((12,)),
+        vm(count, feat, dtype=F32),
+        dma((13,)),
         dma((-(-tok // 256),)),
     ]
     scratch += [dma((tp_count,))] * 2
     scratch += [dma((SPLIT, ep_count))] * 2
     scratch += [dma((ep_count, ep_count))]
-    scratch += [dma((ep_count,))] * 6
+    scratch += [dma((ep_count,))] * 2
+    scratch += [dma((2, ep_count))] * 2
+    scratch += [dma((ep_count,))] * 2
     scratch += [dma((SPLIT, chips))] * 6
     scratch += [dma((chips,))] * 2
     scratch += [dma((SPLIT, ep_count))] * 2
     scratch += [dma((chips,))] * 2
-    return pl.pallas_call(
+    mixer_sum, moe_sum = pl.pallas_call(
         functools.partial(step_kernel, ep_count, tp_count, side, cap),
         out_shape=(
-            jax.ShapeDtypeStruct((tok, feat), BF16),
-            jax.ShapeDtypeStruct((count, feat), BF16),
+            jax.ShapeDtypeStruct((tok, feat), F32),
+            jax.ShapeDtypeStruct((count, feat), F32),
         ),
         in_specs=[VM] * 6 + [ANY] * 12,
-        out_specs=(ANY, VM),
+        out_specs=(ANY, ANY),
         scratch_shapes=scratch,
         compiler_params=pltpu.CompilerParams(
             collective_id=0, has_side_effects=True, vmem_limit_bytes=60 * 1024 * 1024
@@ -867,6 +894,7 @@
         shared_up,
         shared_down,
     )
+    return mixer_sum.astype(BF16), moe_sum.astype(BF16)
 
 
 def solution(mesh):

time: 77.8 us -> 74 us (0.951)
  Pallas kernels: 73.4 us -> 69.7 us
  other arithmetic: 0 us -> 3.41 us
  local copies, waits for them, and re-layouts: 2.96 us -> 0.01 us
    pallas_call x1, Pallas kernels: 73.4 us -> 69.7 us  [local(): pl.pallas_call(functools.partial(step_kernel, ep_count, tp_count, side, c...]
    convert_element_type x0 -> x2, other arithmetic: none -> 3.41 us  [local(): return (mixer_sum.astype(BF16), moe_sum.astype(BF16))]
    unnamed x4 -> x2, local copies, waits for them, and re-layouts: 2.96 us -> 0.01 us
where the time goes in v3:
time: 74 us; the launch traced here: 73.8 us
  Pallas kernels  69.7 us (94%)
  other arithmetic  3.41 us (5%)
    pallas_call x1, Pallas kernels, local(): pl.pallas_call(functools.partial(step_kernel, ep_count, tp_count, side, c...  69.7 us
    convert_element_type x2, other arithmetic, local(): return (mixer_sum.astype(BF16), moe_sum.astype(BF16))  3.41 us

profile of v3, /device:TPU:0, one launch (start us, length us, event | category | flops | bytes accessed | tf_op | source)
XLA Modules:
  0.0 73.8 jit_solution(3863844042862860370)
XLA Ops:
  0.6 69.7 %shard_map.185 = (f32[1024,512]{1,0:T(8,128)}, f32[128,512]{1,0:T(8,128)}) custom-call(f32[2,1024]{1,0:T(2,128)} %ig_ref.1, f32[2,1024]{1,0:T(2,128)} %fg_ref.1, f32[1,256]{1,0:T(1,128)} %bitcast.5, f32[1,4096]{1,0:T(1,128)} %bitcast.4, s32[2,128]{1,0:T(2,128)} %bitcast.6, f32[2,128]{1,0:T(2,128)} %bitcast.7, bf16[1024,128]{1,0:T(8,128)(2,1)} %q_hbm.1, ...), custom_call_target="tpu_custom_call" | custom-call | flops 8999999488 | bytes 30000000 | tf_op jit(solution)/shard_map/pallas_call | solution.py:862
  70.3 0.0 copy-start
  70.3 2.7 %convert_element_type.6 = bf16[1024,512]{1,0:T(8,128)(2,1)} convert(f32[1024,512]{1,0:T(8,128)} %get-tuple-element.4) | non-fusion elementwise | flops 524288 | bytes 3145728 | tf_op jit(solution)/shard_map/convert_element_type | solution.py:897
  73.1 0.0 copy-done
  73.1 0.7 convert_element_type.7
Async XLA Ops:
  70.3 2.7 %copy-start = (f32[128,512]{1,0:T(8,128)S(1)}, f32[128,512]{1,0:T(8,128)}, u32[]{:S(2)}) copy-start(f32[128,512]{1,0:T(8,128)} %get-tuple-element.5) | copy-start | bytes 786436

commit v4 on v3

--- a/solution.py
+++ b/solution.py
@@ -282,6 +282,7 @@
     wx_s,
     wx_r,
     wf_s,
+    wf_r,
     st_s,
     st_r,
     dx_s,
@@ -562,9 +563,13 @@
         ref = wcols.at[pl.ds(part * group, group), origin]
         return remote(ref, ref, wx_s.at[part, peer], wx_r.at[part, origin], (peer, t))
 
-    def wf(part, peer, origin):
-        ref = wcols.at[pl.ds(part * group, group), origin]
-        return remote(ref, ref, wf_s.at[origin, peer], wx_r.at[part, origin], (peer, t))
+    columns = feat // 2
+
+    def wf(part, cut, peer, origin):
+        ref = wcols.at[pl.ds(part * group, group), origin, :, pl.ds(cut * columns, columns)]
+        return remote(
+            ref, ref, wf_s.at[cut, origin, peer], wf_r.at[cut, part, origin], (peer, t)
+        )
 
     paths = ((rowwise, columnwise), (columnwise, rowwise))
 
@@ -653,12 +658,14 @@
     for block in range(chips):
         returned[block, e] = reduced[block, e]
     relay(2, 1)
-    for part, (near, far) in enumerate(paths):
-        for dy, dx in near:
-            origin = ep_peer(dy, dx)
-            wx(part, origin, origin).wait_recv()
-            for fy, fx in far:
-                wf(part, ep_peer(fy, fx), origin).start()
+    for cut in range(2):
+        for part, (near, far) in enumerate(paths):
+            for dy, dx in near:
+                origin = ep_peer(dy, dx)
+                if cut == 0:
+                    wx(part, origin, origin).wait_recv()
+                for fy, fx in far:
+                    wf(part, cut, ep_peer(fy, fx), origin).start()
 
     def zs(to, origin):
         return remote(
@@ -723,52 +730,87 @@
             wx(1, origin, origin).wait_recv()
         elif dx == 0:
             wx(0, origin, origin).wait_recv()
-        else:
-            for part in range(SPLIT):
-                wx(part, origin, origin).wait_recv()
     for part in range(SPLIT):
         for origin in range(chips):
             line_other(part, origin).wait_recv()
     step_rows = tiles(tok, 256)
 
-    @pl.loop(0, tok // step_rows)
-    def _(i):
-        rows = pl.ds(pl.multiple_of(i * step_rows, step_rows), step_rows)
-        total = 0.0
-        for b in range(tp_count):
-            total = total + jnp.dot(
-                mixed[b, rows],
-                wcols[b].reshape(ep_count * share, feat),
-                preferred_element_type=F32,
-            )
-        out_rows[rows] = total
-        pltpu.make_async_copy(out_rows.at[rows], mixer_out.at[rows], out_sem.at[i]).start()
+    for cut in range(2):
+        for dy, dx in around:
+            if dy and dx:
+                for part in range(SPLIT):
+                    origin = ep_peer(dy, dx)
+                    wf(part, cut, origin, origin).wait_recv()
+        cols = pl.ds(cut * columns, columns)
+
+        @pl.loop(0, tok // step_rows)
+        def _(i):
+            rows = pl.ds(pl.multiple_of(i * step_rows, step_rows), step_rows)
+            total = 0.0
+            for b in range(tp_count):
+                total = total + jnp.dot(
+                    mixed[b, rows],
+                    wcols[b, :, :, cut * columns : (cut + 1) * columns].reshape(
+                        ep_count * share, columns
+                    ),
+                    preferred_element_type=F32,
+                )
+            out_rows[rows, cols] = total.astype(BF16)
+            pltpu.make_async_copy(
+                out_rows.at[rows, cols], mixer_out.at[rows, cols], out_sem.at[cut, i]
+            ).start()
 
     total = final[...]
     for k in range(1, chips):
         origin = (z + k) % chips
         zs(origin, origin).wait_recv()
         total = total + part_in[origin].astype(F32)
-    own_rows[...] = total
+    own_rows[...] = total.astype(BF16)
     own_copy = pltpu.make_async_copy(own_rows, moe_out, load_sem.at[len(loads)])
     own_copy.start()
 
     for part, (near, far) in enumerate(paths):
         for dy, dx in near:
             for fy, fx in far:
-                wf(part, ep_peer(fy, fx), ep_peer(dy, dx)).wait_send()
+                for cut in range(2):
+                    wf(part, cut, ep_peer(fy, fx), ep_peer(dy, dx)).wait_send()
     for block in range(chips):
 
         @pl.when(z != block)
         def _():
             zs(block, z).wait_send()
 
-    @pl.loop(0, tok // step_rows)
-    def _(i):
-        rows = pl.ds(pl.multiple_of(i * step_rows, step_rows), step_rows)
-        pltpu.make_async_copy(out_rows.at[rows], mixer_out.at[rows], out_sem.at[i]).wait()
+    for cut in range(2):
+        cols = pl.ds(cut * columns, columns)
+
+        @pl.loop(0, tok // step_rows)
+        def _(i):
+            rows = pl.ds(pl.multiple_of(i * step_rows, step_rows), step_rows)
+            pltpu.make_async_copy(
+                out_rows.at[rows, cols], mixer_out.at[rows, cols], out_sem.at[cut, i]
+            ).wait()
 
     own_copy.wait()
+
+
+def hand_over(pieces, a_ref, b_ref, a_out, b_out, a_buf, b_buf, in_sem, out_sem):
+    size = a_ref.shape[0] // pieces
+    cuts = [pl.ds(i * size, size) for i in range(pieces)]
+    moves = [(a_ref.at[cut], a_buf.at[cut], a_out.at[cut]) for cut in cuts]
+    moves.append((b_ref, b_buf, b_out))
+    loads = [
+        pltpu.make_async_copy(src, buf, in_sem.at[i]) for i, (src, buf, _) in enumerate(moves)
+    ]
+    stores = [
+        pltpu.make_async_copy(buf, dst, out_sem.at[i]) for i, (_, buf, dst) in enumerate(moves)
+    ]
+    for load in loads:
+        load.start()
+    for load, store in zip(loads, stores):
+        load.wait()
+        store.start()
+    for store in stores:
+        store.wait()
 
 
 def local(
@@ -820,7 +862,7 @@
         vm(tok, heads * DV),
         vm(tp_count, tok, heads * DV),
         vm(tp_count, ep_count, share, feat),
-        vm(tok, feat, dtype=F32),
+        vm(tok, feat),
         vm(count, depth),
         vm(tok, held),
         vm(tok, held),
@@ -845,13 +887,13 @@
         vm(chips, count, feat),
         vm(chips, count, feat),
         vm(count, feat, dtype=F32),
-        vm(count, feat, dtype=F32),
+        vm(count, feat),
         dma((13,)),
-        dma((-(-tok // 256),)),
+        dma((2, -(-tok // 256))),
     ]
     scratch += [dma((tp_count,))] * 2
     scratch += [dma((SPLIT, ep_count))] * 2
-    scratch += [dma((ep_count, ep_count))]
+    scratch += [dma((2, ep_count, ep_count)), dma((2, SPLIT, ep_count))]
     scratch += [dma((ep_count,))] * 2
     scratch += [dma((2, ep_count))] * 2
     scratch += [dma((ep_count,))] * 2
@@ -862,8 +904,8 @@
     mixer_sum, moe_sum = pl.pallas_call(
         functools.partial(step_kernel, ep_count, tp_count, side, cap),
         out_shape=(
-            jax.ShapeDtypeStruct((tok, feat), F32),
-            jax.ShapeDtypeStruct((count, feat), F32),
+            jax.ShapeDtypeStruct((tok, feat), BF16),
+            jax.ShapeDtypeStruct((count, feat), BF16),
         ),
         in_specs=[VM] * 6 + [ANY] * 12,
         out_specs=(ANY, ANY),
@@ -894,7 +936,22 @@
         shared_up,
         shared_down,
     )
-    return mixer_sum.astype(BF16), moe_sum.astype(BF16)
+    pieces = 4
+    return pl.pallas_call(
+        functools.partial(hand_over, pieces),
+        out_shape=(
+            jax.ShapeDtypeStruct((tok, feat), BF16),
+            jax.ShapeDtypeStruct((count, feat), BF16),
+        ),
+        in_specs=[ANY] * 2,
+        out_specs=(ANY, ANY),
+        scratch_shapes=[
+            vm(tok, feat),
+            vm(count, feat),
+            dma((pieces + 1,)),
+            dma((pieces + 1,)),
+        ],
+    )(mixer_sum, moe_sum)
 
 
 def solution(mesh):

time: 74 us -> 71.9 us (0.972)
  other arithmetic: 3.41 us -> 0 us
  Pallas kernels: 69.7 us -> 71 us
    convert_element_type x2 -> x0, other arithmetic: 3.41 us -> none  [local(): return (mixer_sum.astype(BF16), moe_sum.astype(BF16))]
    pallas_call x0 -> x1, Pallas kernels: none -> 2.04 us  [local(): pl.pallas_call(functools.partial(hand_over, pieces), out_shape=(jax.Shape...]
where the time goes in v4:
time: 71.9 us; the launch traced here: 71.7 us
  Pallas kernels  71 us (99%)
    pallas_call x1, Pallas kernels, local(): pl.pallas_call(functools.partial(step_kernel, ep_count, tp_count, side, c...  69 us
    pallas_call x1, Pallas kernels, local(): pl.pallas_call(functools.partial(hand_over, pieces), out_shape=(jax.Shape...  2.04 us

profile of v4, /device:TPU:0, one launch (start us, length us, event | category | flops | bytes accessed | tf_op | source)
XLA Modules:
  0.0 71.7 jit_solution(1071729726456736069)
XLA Ops:
  0.6 69.0 %shard_map.185 = (bf16[1024,512]{1,0:T(8,128)(2,1)}, bf16[128,512]{1,0:T(8,128)(2,1)}) custom-call(f32[2,1024]{1,0:T(2,128)} %ig_ref.1, f32[2,1024]{1,0:T(2,128)} %fg_ref.1, f32[1,256]{1,0:T(1,128)} %bitcast.5, f32[1,4096]{1,0:T(1,128)} %bitcast.4, s32[2,128]{1,0:T(2,128)} %bitcast.6, f32[2,128]{1,0:T(2,128)} %bitcast.7, bf16[1024,128]{1,0:T(8,128)(2,1)} %q_hbm.1, ...), custom_call_target="tpu_custom_call" | custom-call | flops 8999999488 | bytes 30000000 | tf_op jit(solution)/shard_map/pallas_call | solution.py:904
  69.6 2.0 %shard_map.186 = (bf16[1024,512]{1,0:T(8,128)(2,1)}, bf16[128,512]{1,0:T(8,128)(2,1)}) custom-call(bf16[1024,512]{1,0:T(8,128)(2,1)} %get-tuple-element.4.a_ref, bf16[128,512]{1,0:T(8,128)(2,1)} %get-tuple-element.5.b_ref), custom_call_target="tpu_custom_call" | custom-call | tf_op jit(solution)/shard_map/pallas_call | solution.py:940
